TPU v7x, 128 devices: a whole 4x4x4 slice. The times are simulated.
128 devices in a mesh: sp: 16 (over z, y), tp: 8 (over x, core).
Axes of the slice: x: 4, y: 4, z: 4, core: 2. Of those that a mesh axis runs over, the one named last changes fastest.
Arguments:
- target: bfloat16 [4096, 2048], P(('sp', 'tp')), may hold values from -6 to 6
- source: bfloat16 [8192, 2048], P(('sp', 'tp')), may hold values from -6 to 6
- target_gain: bfloat16 [2, 2048], replicated, may hold values from 0.099609375 to 1.8984375
- source_gain: bfloat16 [2, 2048], replicated, may hold values from 0.099609375 to 1.8984375
- query_w: bfloat16 [2, 2048, 8192], P(None, None, 'tp'), may hold values from -0.125 to 0.125
- key_w: bfloat16 [2, 2048, 4096], P(None, None, 'tp'), may hold values from -0.125 to 0.125
- value_w: bfloat16 [2, 2048, 4096], P(None, None, 'tp'), may hold values from -0.125 to 0.125
- out_w: bfloat16 [2, 8192, 2048], P(None, 'tp'), may hold values from -0.1875 to 0.1875
- head_temp: float32 [2, 16], P(None, 'tp'), may hold values from 1.5 to 8, as said below
- final_gain: bfloat16 [2048], replicated, may hold values from 0.099609375 to 1.8984375
Outputs:
- result: float32 [4096, 2048], P(('sp', 'tp'))
Inputs may be any that keep to these rules, and one draw needn't show every extreme that they name: `head_temp`: a positive scale for each head's scores.
All inputs are finite; a program needn't handle non-finite values.
Results may differ from a plain program's by a relative error of at most 0.04.
Values may be sent and summed in bfloat16 or wider, within the bound.
A program may use at most 192 MiB of HBM per device.

v0:
```python
import jax
import jax.numpy as jnp
from jax import lax
from jax.sharding import Mesh
from jax.sharding import PartitionSpec as P

HEAD_DIM = 512
TP = ("tp_0", "tp_1")
SP_TP = ("sp", "tp_0", "tp_1")


EPS = 1e-06
FLOOR = -1e30


def laid_out(pieces, dim):
    shape = list(pieces.shape[1:])
    shape[dim] *= pieces.shape[0]
    return jnp.moveaxis(pieces, 0, dim).reshape(shape)


def copy_for_each(shard, axis):
    copies = jnp.broadcast_to(shard, (lax.axis_size(axis), *shard.shape))
    return lax.all_to_all(copies, axis, split_axis=0, concat_axis=0, tiled=True)


def collect(shard, axis, dim):
    return laid_out(copy_for_each(shard, axis), dim)


def cut_rows(length, count):
    hop = length // count
    if hop >= 8:
        hop -= hop % 8
    return [hop * k for k in range(1, count)]


def gather_in_order(shard, axes, order):
    pieces = shard
    for k in order:
        pieces = lax.all_gather(pieces, axes[k])
    done = order[::-1]
    back = [done.index(k) for k in range(len(axes))]
    pieces = pieces.transpose(*back, *range(len(axes), pieces.ndim))
    return pieces.reshape(-1, *shard.shape)


def gather_at_once(shard, axes, dim):
    numbers = list(range(len(axes)))[::-1]
    widest = shard.shape.index(max(shard.shape[:-1] or shard.shape))
    edges = [0, *cut_rows(shard.shape[widest], len(axes)), shard.shape[widest]]
    gathered = []
    for k, (start, end) in enumerate(zip(edges, edges[1:])):
        if end > start:
            share = lax.slice_in_dim(shard, start, end, axis=widest)
            gathered.append(gather_in_order(share, axes, numbers[k:] + numbers[:k]))
    return laid_out(jnp.concatenate(gathered, axis=widest + 1), dim)


def cut_along(shard, dim, count):
    shape = shard.shape
    pieces = shard.reshape(*shape[:dim], count, shape[dim] // count, *shape[dim + 1 :])
    return jnp.moveaxis(pieces, dim, 0)


def summed_on_arrival(shard, axis, dim):
    count = lax.axis_size(axis)
    pieces = lax.all_to_all(cut_along(shard, dim, count), axis, 0, 0, tiled=True)
    return jnp.sum(pieces.astype(jnp.float32), axis=0)


def unit_rows(matrix):
    values = matrix.astype(jnp.float32)
    return values * lax.rsqrt(jnp.mean(values * values, axis=-1, keepdims=True) + EPS)


def per_device(
    target, source, target_gain, source_gain, query_w, key_w, value_w, out_w, head_temp, final_gain
):
    local_heads = query_w.shape[2] // HEAD_DIM
    local_shared = key_w.shape[2] // HEAD_DIM
    group_size = local_heads // local_shared
    shared_width = key_w.shape[2]
    source_gains = source_gain.astype(jnp.float32)
    unit_piece = unit_rows(collect(source, TP, 0))
    outputs = []
    for project_layer_index in range(2):
        project_normed = (unit_piece * source_gains[project_layer_index]).astype(jnp.bfloat16)
        outputs.append(
            jnp.dot(
                project_normed, key_w[project_layer_index], preferred_element_type=jnp.float32
            ).astype(jnp.bfloat16)
        )
        outputs.append(
            jnp.dot(
                project_normed, value_w[project_layer_index], preferred_element_type=jnp.float32
            ).astype(jnp.bfloat16)
        )
    projected = jnp.concatenate(outputs, axis=1)
    hidden_state = target.astype(jnp.float32)
    for layer_index in range(2):
        key_rows = projected[
            :, 2 * layer_index * shared_width : (2 * layer_index + 1) * shared_width
        ]
        value_rows = projected[
            :, (2 * layer_index + 1) * shared_width : (2 * layer_index + 2) * shared_width
        ]
        normed = (unit_rows(hidden_state) * target_gain[layer_index].astype(jnp.float32)).astype(
            jnp.bfloat16
        )
        queries = jnp.dot(
            gather_at_once(normed, TP, 0), query_w[layer_index], preferred_element_type=jnp.float32
        ).astype(jnp.bfloat16)
        row_count = queries.shape[0]
        query_view = queries.reshape(row_count, local_shared, group_size, HEAD_DIM)
        scales = (head_temp[layer_index] * HEAD_DIM ** (-0.5)).reshape(local_shared, group_size)
        start_max = jnp.full((row_count, local_shared, group_size), FLOOR, jnp.float32)
        row_max = start_max
        key_view = lax.all_gather(key_rows, "sp", axis=0, tiled=True).reshape(
            -1, local_shared, HEAD_DIM
        )
        value_view = lax.all_gather(value_rows, "sp", axis=0, tiled=True).reshape(
            -1, local_shared, HEAD_DIM
        )
        scores = jnp.einsum(
            "tkgd,nkd->tkgn", query_view, key_view, preferred_element_type=jnp.float32
        )
        scores = scores * scales[None, :, :, None]
        new_max = jnp.maximum(row_max, jnp.max(scores, axis=-1))
        exponent = jnp.exp(scores - new_max[..., None])
        row_total = jnp.sum(exponent, axis=-1)
        accumulated = jnp.einsum(
            "tkgn,nkd->tkgd",
            exponent.astype(jnp.bfloat16),
            value_view,
            preferred_element_type=jnp.float32,
        )
        row_max, row_total, accumulated = (new_max, row_total, accumulated)
        attended = (accumulated / row_total[..., None]).astype(jnp.bfloat16)
        flat_heads = attended.reshape(row_count, local_heads * HEAD_DIM)
        mixed = summed_on_arrival(
            jnp.dot(flat_heads, out_w[layer_index], preferred_element_type=jnp.float32).astype(
                jnp.bfloat16
            ),
            TP,
            0,
        )
        hidden_state = hidden_state + mixed
    return unit_rows(hidden_state) * final_gain.astype(jnp.float32)


def solution(mesh):
    split = Mesh(mesh.devices.reshape(mesh.shape["sp"], 4, 2), ("sp", "tp_0", "tp_1"))
    in_specs = (
        P(SP_TP, None),
        P(SP_TP, None),
        P(),
        P(),
        P(None, None, TP),
        P(None, None, TP),
        P(None, None, TP),
        P(None, TP, None),
        P(None, TP),
        P(),
    )
    out_specs = P(SP_TP, None)
    return jax.shard_map(
        per_device, mesh=split, in_specs=in_specs, out_specs=out_specs, check_vma=False
    )
```

profile of v0, /device:TPU:0, one launch (start us, length us, event | category | flops | bytes accessed | tf_op | source)
XLA Modules:
  0.0 381.4 jit_solution(2791178233135704088)
XLA Ops:
  6.5 2.6 broadcast_in_dim.2
  9.1 4.4 %all-to-all-start = ((bf16[8,64,2048]{2,1,0:T(8,128)(2,1)}), bf16[8,64,2048]{2,1,0:T(8,128)(2,1)S(1)}, u32[]{:S(2)}, u32[]{:S(2)}) async-start(bf16[8,64,2048]{2,1,0:T(8,128)(2,1)} %broadcast_in_dim.2), calls=%async_computation | async-start | bytes 4194304 | tf_op jit(solution)/shard_map/all_to_all | solution.py:24
  13.5 0.0 all-gather.15.cloned.1.call-start
  13.6 0.0 copy-done.3
  13.6 27.1 %all-to-all-done = bf16[8,64,2048]{2,1,0:T(8,128)(2,1)S(1)} async-done(((bf16[8,64,2048]{2,1,0:T(8,128)(2,1)}), bf16[8,64,2048]{2,1,0:T(8,128)(2,1)S(1)}, u32[]{:S(2)}, u32[]{:S(2)}) %all-to-all-start) | async-done | bytes 2097184 | tf_op jit(solution)/shard_map/all_to_all | solution.py:24
  40.7 0.5 fusion.26
  41.2 2.1 fusion.24
  43.3 1.3 copy-done.2
  44.6 0.0 copy-done.7
  44.6 2.1 fusion.70
  46.7 0.0 all-gather.15.cloned.1.call-update
  46.7 0.0 all-gather.13.cloned.1.call-start
  46.8 4.4 %fusion.67 = bf16[512,512]{1,0:T(8,128)(2,1)} fusion(bf16[512,2048]{1,0:T(8,128)(2,1)} %bitcast.231, bf16[2,2048,512]{2,1,0:T(8,128)(2,1)} %param.16), kind=kOutput, calls=%fused_computation.63 | convolution fusion | flops 1074003968 | bytes 4718592 | tf_op jit(solution)/shard_map/dot_general | solution.py:95
  51.2 0.0 all-gather.13.cloned.1.call-update
  51.2 0.0 all-gather.19.cloned.1.call-start
  51.3 0.0 copy-done.1
  51.3 3.7 fusion.76
  54.9 0.0 all-gather.19.cloned.1.call-update
  55.0 0.0 copy-start.6
  55.0 0.0 all-gather.17.cloned.1.call-start
  55.0 3.7 fusion.73
  58.7 0.0 all-gather.17.cloned.1.call-update
  58.7 0.0 copy-done
  58.7 0.1 fusion.109
  58.9 0.0 copy-done.4
  58.9 0.1 fusion.111
  59.0 12.4 %all-gather.2 = bf16[64,2048]{1,0:T(8,128)(2,1)S(1)} all-gather(bf16[16,2048]{1,0:T(8,128)(2,1)S(1)} %get-tuple-element.10), channel_id=4, replica_groups=mesh['sp'=16,'tp_0'=4,'tp_1'=2] {'tp_0'}, dimensions={0}, use_global_device_ids=true | all-gather | bytes 327680 | tf_op jit(solution)/shard_map/all_gather | solution.py:41
  71.4 2.2 all-gather.3
  73.6 1.9 all-gather
  75.5 13.5 %all-gather.1 = bf16[8,16,2048]{2,1,0:T(8,128)(2,1)S(1)} all-gather(bf16[2,16,2048]{2,1,0:T(8,128)(2,1)S(1)} %bitcast.237), channel_id=3, replica_groups=mesh['sp'=16,'tp_0'=4,'tp_1'=2] {'tp_0'}, dimensions={0}, use_global_device_ids=true | all-gather | bytes 655360 | tf_op jit(solution)/shard_map/all_gather | solution.py:41
  89.0 0.0 copy-done.6
  89.0 0.1 pad_maximum_fusion
  89.1 3.5 fusion.79
  92.5 25.8 %all-gather.15.cloned.1.call-done = bf16[8192,512]{1,0:T(8,128)(2,1)} async-done(((bf16[512,512]{1,0:T(8,128)(2,1)}), bf16[8192,512]{1,0:T(8,128)(2,1)}) %all-gather.15.cloned.1.call-update) | async-done | bytes 8388624 | tf_op jit(solution)/shard_map/all_gather | solution.py:119
  118.4 11.7 %bitcast_reduce_fusion.1 = (f32[256,2]{0,1:T(2,128)S(1)}, f32[8192,256,2]{1,0,2:T(8,128)}) fusion(f32[2]{0:T(128)S(1)} %get-tuple-element.16, bf16[32,2,8,512]{3,2,1,0:T(8,128)(2,1)S(1)} %bitcast.246, bf16[8192,512]{1,0:T(8,128)(2,1)} %all-gather.15.cloned.1.call-done), kind=kOutput, calls=%fused_computation.5 | convolution fusion | flops 4303355392 | bytes 25692168 | tf_op jit(solution)/shard_map/tkgd,nkd->tkgn/dot_general | solution.py:125
  130.0 8.8 %fusion.2 = f32[256,2]{0,1:T(2,128)S(1)} fusion(f32[8192,256,2]{1,0,2:T(8,128)} %get-tuple-element.18, f32[256,2]{0,1:T(2,128)S(1)} %broadcast_maximum_fusion.1, f32[2]{0:T(128)S(1)} %get-tuple-element.16), kind=kLoop, calls=%fused_computation.8 | loop fusion | flops 12582400 | bytes 16781320 | tf_op jit(solution)/shard_map/reduce_sum | solution.py:131
  138.8 52.2 %all-gather.13.cloned.1.call-done = bf16[8192,512]{1,0:T(8,128)(2,1)} async-done(((bf16[512,512]{1,0:T(8,128)(2,1)}), bf16[8192,512]{1,0:T(8,128)(2,1)}) %all-gather.13.cloned.1.call-update) | async-done | bytes 8388624 | tf_op jit(solution)/shard_map/all_gather | solution.py:122
  191.0 12.8 %fusion.100 = bf16[1,512,256,2]{2,1,3,0:T(8,128)(2,1)S(1)} fusion(f32[8192,256,2]{1,0,2:T(8,128)} %get-tuple-element.18, f32[256,2]{0,1:T(2,128)S(1)} %broadcast_maximum_fusion.1, f32[2]{0:T(128)S(1)} %get-tuple-element.16, bf16[8192,512]{1,0:T(8,128)(2,1)} %all-gather.13.cloned.1.call-done, f32[256,2]{0,1:T(2,128)S(1)} %fusion.2), kind=kOutput, calls=%fused_computation.72 | convolution fusion | flops 4308074496 | bytes 25694216 | tf_op jit(solution)/shard_map/tkgn,nkd->tkgd/dot_general | solution.py:132
  203.9 0.0 slice-start
  203.9 3.6 fusion.39
  207.5 0.0 slice-start.1
  207.5 20.3 %all_to_all.15 = bf16[8,32,2048]{2,1,0:T(8,128)(2,1)S(1)} all-to-all(bf16[8,32,2048]{2,1,0:T(8,128)(2,1)S(1)} %bitcast.236), channel_id=1, replica_groups=mesh['sp'=16,'tp_0'=4,'tp_1'=2] {'tp_0','tp_1'}, dimensions={0} | all-to-all | bytes 2097152 | tf_op jit(solution)/shard_map/all_to_all | solution.py:68
  227.8 0.1 convert_reduce_fusion.1
  227.9 0.1 multiply_reduce_fusion.1
  228.1 0.1 multiply_convert_fusion
  228.2 12.3 %all-gather.6 = bf16[64,2048]{1,0:T(8,128)(2,1)S(1)} all-gather(bf16[16,2048]{1,0:T(8,128)(2,1)S(1)} %get-tuple-element.8), channel_id=8, replica_groups=mesh['sp'=16,'tp_0'=4,'tp_1'=2] {'tp_0'}, dimensions={0}, use_global_device_ids=true | all-gather | bytes 327680 | tf_op jit(solution)/shard_map/all_gather | solution.py:41
  240.5 2.2 all-gather.7
  242.7 1.9 all-gather.4
  244.6 13.0 %all-gather.5 = bf16[8,16,2048]{2,1,0:T(8,128)(2,1)S(1)} all-gather(bf16[2,16,2048]{2,1,0:T(8,128)(2,1)S(1)} %bitcast.238), channel_id=7, replica_groups=mesh['sp'=16,'tp_0'=4,'tp_1'=2] {'tp_0'}, dimensions={0}, use_global_device_ids=true | all-gather | bytes 655360 | tf_op jit(solution)/shard_map/all_gather | solution.py:41
  257.6 0.1 pad_maximum_fusion.1
  257.7 1.3 fusion.82
  259.0 4.8 %all-gather.19.cloned.1.call-done = bf16[8192,512]{1,0:T(8,128)(2,1)} async-done(((bf16[512,512]{1,0:T(8,128)(2,1)}), bf16[8192,512]{1,0:T(8,128)(2,1)}) %all-gather.19.cloned.1.call-update) | async-done | bytes 8388624 | tf_op jit(solution)/shard_map/all_gather | solution.py:119
  263.7 11.7 %bitcast_reduce_fusion = (f32[256,2]{0,1:T(2,128)S(1)}, f32[8192,256,2]{1,0,2:T(8,128)}) fusion(f32[2]{0:T(128)S(1)} %get-tuple-element.15, bf16[32,2,8,512]{3,2,1,0:T(8,128)(2,1)S(1)} %bitcast.245, bf16[8192,512]{1,0:T(8,128)(2,1)} %all-gather.19.cloned.1.call-done), kind=kOutput, calls=%fused_computation.1 | convolution fusion | flops 4303355392 | bytes 25692168 | tf_op jit(solution)/shard_map/tkgd,nkd->tkgn/dot_general | solution.py:125
  275.5 8.7 %fusion.4 = f32[256,2]{0,1:T(2,128)S(1)} fusion(f32[8192,256,2]{1,0,2:T(8,128)} %get-tuple-element.20, f32[256,2]{0,1:T(2,128)S(1)} %broadcast_maximum_fusion, f32[2]{0:T(128)S(1)} %get-tuple-element.15), kind=kLoop, calls=%fused_computation.10 | loop fusion | flops 12582400 | bytes 16781320 | tf_op jit(solution)/shard_map/reduce_sum | solution.py:131
  284.2 52.1 %all-gather.17.cloned.1.call-done = bf16[8192,512]{1,0:T(8,128)(2,1)} async-done(((bf16[512,512]{1,0:T(8,128)(2,1)}), bf16[8192,512]{1,0:T(8,128)(2,1)}) %all-gather.17.cloned.1.call-update) | async-done | bytes 8388624 | tf_op jit(solution)/shard_map/all_gather | solution.py:122
  336.3 12.8 %fusion.90 = bf16[1,512,256,2]{2,1,3,0:T(8,128)(2,1)S(1)} fusion(f32[8192,256,2]{1,0,2:T(8,128)} %get-tuple-element.20, f32[256,2]{0,1:T(2,128)S(1)} %broadcast_maximum_fusion, f32[2]{0:T(128)S(1)} %get-tuple-element.15, bf16[8192,512]{1,0:T(8,128)(2,1)} %all-gather.17.cloned.1.call-done, f32[256,2]{0,1:T(2,128)S(1)} %fusion.4), kind=kOutput, calls=%fused_computation.70 | convolution fusion | flops 4308074496 | bytes 25694216 | tf_op jit(solution)/shard_map/tkgn,nkd->tkgd/dot_general | solution.py:132
  349.1 0.0 copy-start.5
  349.1 4.4 %fusion.42 = bf16[256,2048]{1,0:T(8,128)(2,1)} fusion(bf16[256,1024]{0,1:T(8,128)(2,1)S(1)} %bitcast.248, bf16[2,1024,2048]{2,1,0:T(8,128)(2,1)} %param.17), kind=kOutput, calls=%fused_computation.46 | convolution fusion | flops 1074266112 | bytes 5767168 | tf_op jit(solution)/shard_map/dot_general | solution.py:142
  353.5 4.3 %all-to-all-start.2 = ((bf16[8,32,2048]{2,1,0:T(8,128)(2,1)}), bf16[8,32,2048]{2,1,0:T(8,128)(2,1)S(1)}, u32[]{:S(2)}, u32[]{:S(2)}) async-start(bf16[8,32,2048]{2,1,0:T(8,128)(2,1)} %bitcast.45), calls=%async_computation.2 | async-start | bytes 2097152 | tf_op jit(solution)/shard_map/all_to_all | solution.py:68
  357.8 0.0 copy-done.5
  357.8 15.9 %all-to-all-done.2 = bf16[8,32,2048]{2,1,0:T(8,128)(2,1)S(1)} async-done(((bf16[8,32,2048]{2,1,0:T(8,128)(2,1)}), bf16[8,32,2048]{2,1,0:T(8,128)(2,1)S(1)}, u32[]{:S(2)}, u32[]{:S(2)}) %all-to-all-start.2) | async-done | bytes 1048608 | tf_op jit(solution)/shard_map/all_to_all | solution.py:68
  373.7 0.1 convert_reduce_fusion
  373.9 0.2 multiply_reduce_fusion
  374.0 0.8 multiply_multiply_fusion
  (23 shorter events, 0.2 us)
Async XLA Ops:
  6.5 7.0 %copy-start.3 = (bf16[2,2048]{1,0:T(2,128)(2,1)S(1)}, bf16[2,2048]{1,0:T(2,128)(2,1)}, u32[]{:S(2)}) copy-start(bf16[2,2048]{1,0:T(2,128)(2,1)} %param.13) | copy-start | bytes 24580
  9.1 31.6 %all-to-all-start = ((bf16[8,64,2048]{2,1,0:T(8,128)(2,1)}), bf16[8,64,2048]{2,1,0:T(8,128)(2,1)S(1)}, u32[]{:S(2)}, u32[]{:S(2)}) async-start(bf16[8,64,2048]{2,1,0:T(8,128)(2,1)} %broadcast_in_dim.2), calls=%async_computation | async-start | bytes 4194304 | tf_op jit(solution)/shard_map/all_to_all | solution.py:24
  13.5 104.8 %all-gather.15.cloned.1.call-start = ((), (), s32[]{:S(2)}) async-start(), calls=%async_computation.4 | async-start | bytes 8912896 | tf_op jit(solution)/shard_map/all_gather | solution.py:119
  40.7 3.9 %copy-start.7 = (bf16[2,2048,512]{2,1,0:T(8,128)(2,1)S(1)}, bf16[2,2048,512]{2,1,0:T(8,128)(2,1)}, u32[]{:S(2)}) copy-start(bf16[2,2048,512]{2,1,0:T(8,128)(2,1)} %param.15) | copy-start | bytes 12582916
  43.3 1.3 copy-start.2
  46.7 4.6 %copy-start.1 = (bf16[8,64,2048]{2,1,0:T(8,128)(2,1)S(1)}, bf16[8,64,2048]{2,1,0:T(8,128)(2,1)}, u32[]{:S(2)}) copy-start(bf16[8,64,2048]{2,1,0:T(8,128)(2,1)} %get-tuple-element.6) | copy-start | bytes 6291460
  46.7 144.3 %all-gather.13.cloned.1.call-start = ((), (), s32[]{:S(2)}) async-start(), calls=%async_computation.3 | async-start | bytes 8912896 | tf_op jit(solution)/shard_map/all_gather | solution.py:122
  51.2 212.5 %all-gather.19.cloned.1.call-start = ((), (), s32[]{:S(2)}) async-start(), calls=%async_computation.6 | async-start | bytes 8912896 | tf_op jit(solution)/shard_map/all_gather | solution.py:119
  54.9 3.8 copy-start
  54.9 4.0 %copy-start.4 = (bf16[2,2048]{1,0:T(2,128)(2,1)S(1)}, bf16[2,2048]{1,0:T(2,128)(2,1)}, u32[]{:S(2)}) copy-start(bf16[2,2048]{1,0:T(2,128)(2,1)} %param.12) | copy-start | bytes 24580
  55.0 34.0 %copy-start.6 = (f32[2,2]{1,0:T(2,128)S(1)}, f32[2,2]{1,0:T(2,128)}, u32[]{:S(2)}) copy-start(f32[2,2]{1,0:T(2,128)} %param.18) | copy-start | bytes 52
  55.0 281.3 %all-gather.17.cloned.1.call-start = ((), (), s32[]{:S(2)}) async-start(), calls=%async_computation.5 | async-start | bytes 8912896 | tf_op jit(solution)/shard_map/all_gather | solution.py:122
  203.9 53.8 %slice-start = ((s8[8388608]{0:T(1024)(128)(4,1)}), s8[4194304]{0:T(1024)(128)(4,1)S(1)}, s32[]{:S(2)}) async-start(s8[8388608]{0:T(1024)(128)(4,1)} %bitcast.243), calls=%async_computation.7 | async-start | bytes 8388608
  207.5 50.2 %slice-start.1 = ((s8[8388608]{0:T(1024)(128)(4,1)}), s8[4194304]{0:T(1024)(128)(4,1)S(1)}, s32[]{:S(2)}) async-start(s8[8388608]{0:T(1024)(128)(4,1)} %bitcast.243), calls=%async_computation.8 | async-start | bytes 8388608
  349.1 8.7 %copy-start.5 = (bf16[2048]{0:T(1024)(128)(2,1)S(1)}, bf16[2048]{0:T(1024)(128)(2,1)}, u32[]{:S(2)}) copy-start(bf16[2048]{0:T(1024)(128)(2,1)} %param.19) | copy-start | bytes 12292
  353.5 20.2 %all-to-all-start.2 = ((bf16[8,32,2048]{2,1,0:T(8,128)(2,1)}), bf16[8,32,2048]{2,1,0:T(8,128)(2,1)S(1)}, u32[]{:S(2)}, u32[]{:S(2)}) async-start(bf16[8,32,2048]{2,1,0:T(8,128)(2,1)} %bitcast.45), calls=%async_computation.2 | async-start | bytes 2097152 | tf_op jit(solution)/shard_map/all_to_all | solution.py:68
Sparse Core Ops, SparseCore 0:
  46.9 71.4 all-gather.14
  120.5 70.5 all-gather.12
  193.2 70.5 all-gather.18
  265.7 70.5 all-gather.16
where the time goes:
time: 382 us; the launch traced here: 381 us
  waiting for transfers between devices  178 us (47%)
  blocking collectives  79.5 us (21%)
  matrix products  75.6 us (20%)
  other arithmetic  22 us (6%)
  between operations  13.4 us (4%)
  starting transfers between devices  8.83 us (2%)
  local copies, waits for them, and re-layouts  4.03 us (1%)
    all_gather x2, waiting for transfers between devices, per_device(): lax.all_gather(value_rows, 'sp', axis=0, tiled=True)  104 us
    all_gather x8, blocking collectives, gather_in_order(): pieces = lax.all_gather(pieces, axes[k])  59.2 us
    all_gather x2, waiting for transfers between devices, per_device(): lax.all_gather(key_rows, 'sp', axis=0, tiled=True)  30.6 us
    all_to_all x1, waiting for transfers between devices, copy_for_each(): return lax.all_to_all(copies, axis, split_axis=0, concat_axis=0, tiled=True)  27.1 us
    dot_general x2, matrix products, per_device(): jnp.einsum('tkgn,nkd->tkgd', exponent.astype(jnp.bfloat16), value_view, p...  25.6 us
    dot_general x2, matrix products, per_device(): jnp.einsum('tkgd,nkd->tkgn', query_view, key_view, preferred_element_type...  23.4 us
    all_to_all x1, blocking collectives, summed_on_arrival(): lax.all_to_all(cut_along(shard, dim, count), axis, 0, 0, tiled=True)  20.3 us
    reduce_sum x2, other arithmetic, per_device(): row_total = jnp.sum(exponent, axis=-1)  17.5 us
  transfers between devices with their start and end apart: 6, of which 6 were waited for; matrix products, arithmetic and copies ran while one was open for 20% of the time, Pallas kernels for 0%

commit v1 on v0

v1 whole, which is shorter than its diff:
```python
import jax
import jax.numpy as jnp
from jax import lax
from jax.sharding import Mesh
from jax.sharding import PartitionSpec as P

HEAD_DIM = 512
EPS = 1e-06
ROWS = ("z", "y", "x", "c")
SRC_PLANE = ("y", "x", "c")
TGT_PLANE = ("z", "x", "c")
TP = ("x", "c")


def unit_rows(matrix):
    values = matrix.astype(jnp.float32)
    return values * lax.rsqrt(jnp.mean(values * values, axis=-1, keepdims=True) + EPS)


def per_device(
    target, source, target_gain, source_gain, query_w, key_w, value_w, out_w, head_temp, final_gain
):
    local_heads = query_w.shape[2] // HEAD_DIM
    src = lax.all_gather(source, SRC_PLANE, axis=0, tiled=True)
    unit_src = unit_rows(src)
    hidden = target.astype(jnp.float32)
    for l in range(2):
        normed_src = (unit_src * source_gain[l].astype(jnp.float32)).astype(jnp.bfloat16)
        k = jnp.dot(normed_src, key_w[l], preferred_element_type=jnp.float32).astype(jnp.bfloat16)
        v = jnp.dot(normed_src, value_w[l], preferred_element_type=jnp.float32).astype(jnp.bfloat16)
        normed = (unit_rows(hidden) * target_gain[l].astype(jnp.float32)).astype(jnp.bfloat16)
        full = lax.all_gather(normed, TGT_PLANE, axis=0, tiled=True)
        q = jnp.dot(full, query_w[l], preferred_element_type=jnp.float32).astype(jnp.bfloat16)
        rows = q.shape[0]
        q = q.reshape(rows, local_heads, HEAD_DIM)
        scales = head_temp[l] * HEAD_DIM ** (-0.5)
        s = jnp.einsum("thd,nd->htn", q, k, preferred_element_type=jnp.float32)
        s = s * scales[:, None, None]
        m = jnp.max(s, axis=-1)
        e = jnp.exp(s - m[..., None])
        t = jnp.sum(e, axis=-1)
        o = jnp.einsum("htn,nd->htd", e.astype(jnp.bfloat16), v, preferred_element_type=jnp.float32)
        stats = lax.all_gather(jnp.stack([m, t]), "z")
        gm = jnp.max(stats[:, 0], axis=0)
        gt = jnp.sum(stats[:, 1] * jnp.exp(stats[:, 0] - gm[None]), axis=0)
        o = o * (jnp.exp(m - gm) / gt)[..., None]
        o = o.astype(jnp.bfloat16)
        flat = o.transpose(1, 0, 2).reshape(rows, local_heads * HEAD_DIM)
        part = jnp.dot(flat, out_w[l], preferred_element_type=jnp.float32).astype(jnp.bfloat16)
        mixed = lax.psum_scatter(part, TGT_PLANE, scatter_dimension=0, tiled=True)
        hidden = hidden + mixed.astype(jnp.float32)
    return unit_rows(hidden) * final_gain.astype(jnp.float32)


def solution(mesh):
    split = Mesh(mesh.devices.reshape(4, 4, 4, 2), ROWS)
    in_specs = (
        P(ROWS, None),
        P(ROWS, None),
        P(),
        P(),
        P(None, None, TP),
        P(None, None, TP),
        P(None, None, TP),
        P(None, TP, None),
        P(None, TP),
        P(),
    )
    return jax.shard_map(
        per_device, mesh=split, in_specs=in_specs, out_specs=P(ROWS, None), check_vma=False
    )
```

time: 382 us -> 473 us (1.24)
  waiting for transfers between devices: 178 us -> 302 us
  blocking collectives: 79.5 us -> 24.2 us
  matrix products: 75.6 us -> 94.7 us
  other arithmetic: 22 us -> 33 us
  starting transfers between devices: 8.83 us -> 0.17 us
    reduce_scatter x0 -> x2, waiting for transfers between devices: none -> 163 us  [per_device(): mixed = lax.psum_scatter(part, TGT_PLANE, scatter_dimension=0, tiled=True)]
    all_to_all x2 -> x0, waiting for transfers between devices: 43 us -> none  [the longest x1 27.1 us: copy_for_each(): return lax.all_to_all(copies, axis, split_axis=0, concat_axis=0, tiled=True)]
    all_gather x8 -> x2, blocking collectives: 59.2 us -> 24.2 us  [per_device(): stats = lax.all_gather(jnp.stack([m, t]), 'z')]
    all_to_all x1 -> x0, blocking collectives: 20.3 us -> none  [summed_on_arrival(): lax.all_to_all(cut_along(shard, dim, count), axis, 0, 0, tiled=True)]
    dot_general x12 -> x8, matrix products: 75.6 us -> 94.7 us  [the longest x2 31.3 us: per_device(): s = jnp.einsum('thd,nd->htn', q, k, preferred_element_type=jnp.float32)]
    all_to_all x2 -> x0, starting transfers between devices: 8.67 us -> none  [the longest x1 4.41 us: copy_for_each(): return lax.all_to_all(copies, axis, split_axis=0, concat_axis=0, tiled=True)]
    reduce_sum x4, other arithmetic: 0.93 us -> 8.24 us  [unit_rows(): jnp.mean(values * values, axis=-1, keepdims=True) + EPS]
    all_gather x4 -> x3, waiting for transfers between devices: 135 us -> 138 us  [the longest x2 92 us: per_device(): full = lax.all_gather(normed, TGT_PLANE, axis=0, tiled=True)]
  transfers between devices with their start and end apart: 6 -> 5, of which waited for: 6 -> 5; matrix products, arithmetic and copies ran while one was open for 20% -> 2% of each run, Pallas kernels for 0% -> 0%
where the time goes in v1:
time: 473 us; the launch traced here: 468 us
  waiting for transfers between devices  302 us (64%)
  matrix products  94.7 us (20%)
  other arithmetic  33 us (7%)
  blocking collectives  24.2 us (5%)
  between operations  13.5 us (3%)
    reduce_scatter x2, waiting for transfers between devices, per_device(): mixed = lax.psum_scatter(part, TGT_PLANE, scatter_dimension=0, tiled=True)  163 us
    all_gather x2, waiting for transfers between devices, per_device(): full = lax.all_gather(normed, TGT_PLANE, axis=0, tiled=True)  92 us
    all_gather x1, waiting for transfers between devices, per_device(): src = lax.all_gather(source, SRC_PLANE, axis=0, tiled=True)  46.2 us
    dot_general x2, matrix products, per_device(): s = jnp.einsum('thd,nd->htn', q, k, preferred_element_type=jnp.float32)  31.3 us
    dot_general x2, matrix products, per_device(): jnp.einsum('htn,nd->htd', e.astype(jnp.bfloat16), v, preferred_element_ty...  30.6 us
    all_gather x2, blocking collectives, per_device(): stats = lax.all_gather(jnp.stack([m, t]), 'z')  24.2 us
    reduce_sum x2, other arithmetic, per_device(): t = jnp.sum(e, axis=-1)  17.1 us
    dot_general x2, matrix products, per_device(): jnp.dot(flat, out_w[l], preferred_element_type=jnp.float32)  16.8 us
  transfers between devices with their start and end apart: 5, of which 5 were waited for; matrix products, arithmetic and copies ran while one was open for 2% of the time, Pallas kernels for 0%

profile of v1, /device:TPU:0, one launch (start us, length us, event | category | flops | bytes accessed | tf_op | source)
XLA Modules:
  0.0 467.8 jit_solution(16193505409996494158)
XLA Ops:
  6.5 0.0 all-gather.8.cloned.1.call-start
  6.5 0.8 slice_convert_fusion
  7.3 1.0 fusion.85
  8.4 1.7 fusion.87
  10.0 0.0 all-gather.8.cloned.1.call-update
  10.1 0.0 all-gather.6.cloned.1.call-start
  10.1 0.7 all-gather.6.cloned.1.call-update
  10.8 0.0 reduce-scatter.3.cloned.1.call-start
  10.9 0.8 multiply_bitcast_fusion
  11.6 0.8 slice_convert_fusion.1
  12.4 46.5 %all-gather.8.cloned.1.call-done = bf16[1024,2048]{1,0:T(8,128)(2,1)} async-done(((bf16[32,2048]{1,0:T(8,128)(2,1)}), bf16[1024,2048]{1,0:T(8,128)(2,1)}) %all-gather.8.cloned.1.call-update) | async-done | bytes 4194320 | tf_op jit(solution)/shard_map/all_gather | solution.py:32
  58.9 8.0 %fusion.69 = bf16[1024,1024]{0,1:T(8,128)(2,1)S(1)} fusion(bf16[1024,2048]{1,0:T(8,128)(2,1)} %all-gather.8.cloned.1.call-done, bf16[2,2048,1024]{2,1,0:T(8,128)(2,1)} %param.14), kind=kOutput, calls=%fused_computation.57 | convolution fusion | flops 4296015872 | bytes 10485760 | tf_op jit(solution)/shard_map/dot_general | solution.py:33
  66.9 46.2 %all-gather.6.cloned.1.call-done = bf16[2048,2048]{1,0:T(8,128)(2,1)} async-done(((bf16[64,2048]{1,0:T(8,128)(2,1)}), bf16[2048,2048]{1,0:T(8,128)(2,1)}) %all-gather.6.cloned.1.call-update) | async-done | bytes 8388624 | tf_op jit(solution)/shard_map/all_gather | solution.py:24
  113.1 5.1 %fusion.4 = f32[2048]{0:T(1024)S(1)} fusion(bf16[2048,2048]{1,0:T(8,128)(2,1)} %all-gather.6.cloned.1.call-done), kind=kLoop, calls=%fused_computation.6 | loop fusion | flops 12580864 | bytes 8396800 | tf_op jit(solution)/shard_map/reduce_sum | solution.py:17
  118.2 15.8 %bitcast_reduce_fusion.1 = (f32[2,1024]{1,0:T(2,128)S(1)}, f32[2048,1024,2]{1,0,2:T(8,128)}) fusion(f32[2]{0:T(128)S(1)} %get-tuple-element.10, bf16[1024,2,512]{0,2,1:T(8,128)(2,1)S(1)} %bitcast.168, bf16[2048,2048]{1,0:T(8,128)(2,1)} %all-gather.6.cloned.1.call-done, f32[2048]{0:T(1024)S(1)} %bitcast.166, f32[2048]{0:T(1024)S(1)} %add_rsqrt_fusion, ...), kind=kOutput, calls=%fused_computation.11 | convolution fusion | flops 8616146944 | bytes 29384712 | tf_op jit(solution)/shard_map/thd,nd->htn/dot_general | solution.py:37
  134.0 8.6 %fusion.7 = f32[2,1024]{1,0:T(2,128)S(1)} fusion(f32[2048,1024,2]{1,0,2:T(8,128)} %get-tuple-element.12, f32[2,1024]{1,0:T(2,128)S(1)} %get-tuple-element.11, f32[2]{0:T(128)S(1)} %get-tuple-element.10), kind=kLoop, calls=%fused_computation.13 | loop fusion | flops 12580864 | bytes 16793608 | tf_op jit(solution)/shard_map/reduce_sum | solution.py:41
  142.6 12.3 %all-gather = f32[8,2,1024]{2,1,0:T(2,128)S(1)} all-gather(f32[2,2,1024]{2,1,0:T(2,128)S(1)} %pad_maximum_fusion), channel_id=2, replica_groups=mesh['z'=4,'y'=4,'x'=4,'c'=2] {'z'}, dimensions={0}, use_global_device_ids=true | all-gather | bytes 81920 | tf_op jit(solution)/shard_map/all_gather | solution.py:43
  155.0 15.2 %fusion.26 = bf16[1024,2,512]{0,2,1:T(8,128)(2,1)S(1)} fusion(f32[2048,1024,2]{1,0,2:T(8,128)} %get-tuple-element.12, f32[2,1024]{1,0:T(2,128)S(1)} %get-tuple-element.11, f32[2]{0:T(128)S(1)} %get-tuple-element.10, bf16[2048,2048]{1,0:T(8,128)(2,1)} %all-gather.6.cloned.1.call-done, f32[2048]{0:T(1024)S(1)} %bitcast.167, f32[2048]{0:T(1024)S(1)} %add_rsqrt_fusion, ...), kind=kOutput, calls=%fused_computation.32 | convolution fusion | flops 8622440448 | bytes 29392904 | tf_op jit(solution)/shard_map/htn,nd->htd/dot_general | solution.py:42
  170.3 0.0 copy-start
  170.3 8.4 %fusion.33 = bf16[1024,2048]{1,0:T(8,128)(2,1)} fusion(bf16[1024,1024]{0,1:T(8,128)(2,1)S(1)} %bitcast.170, bf16[2,1024,2048]{2,1,0:T(8,128)(2,1)} %param.17), kind=kOutput, calls=%fused_computation.39 | convolution fusion | flops 4297064448 | bytes 10485760 | tf_op jit(solution)/shard_map/dot_general | solution.py:49
  178.7 0.0 reduce-scatter.3.cloned.1.call-update
  178.7 0.0 all-gather.10.cloned.1.call-start
  178.7 81.5 %reduce-scatter.3.cloned.1.call-done = bf16[32,2048]{1,0:T(8,128)(2,1)} async-done(((bf16[1024,2048]{1,0:T(8,128)(2,1)}), bf16[32,2048]{1,0:T(8,128)(2,1)}) %reduce-scatter.3.cloned.1.call-update) | async-done | bytes 131088 | tf_op jit(solution)/shard_map/reduce_scatter | solution.py:50
  260.3 0.0 copy-done
  260.3 1.1 multiply_reduce_fusion.1
  261.3 1.7 multiply_convert_fusion
  263.0 0.0 all-gather.10.cloned.1.call-update
  263.0 0.0 reduce-scatter.5.cloned.1.call-start
  263.1 45.6 %all-gather.10.cloned.1.call-done = bf16[1024,2048]{1,0:T(8,128)(2,1)} async-done(((bf16[32,2048]{1,0:T(8,128)(2,1)}), bf16[1024,2048]{1,0:T(8,128)(2,1)}) %all-gather.10.cloned.1.call-update) | async-done | bytes 4194320 | tf_op jit(solution)/shard_map/all_gather | solution.py:32
  308.6 8.0 %fusion.72 = bf16[1024,1024]{0,1:T(8,128)(2,1)S(1)} fusion(bf16[1024,2048]{1,0:T(8,128)(2,1)} %all-gather.10.cloned.1.call-done, bf16[2,2048,1024]{2,1,0:T(8,128)(2,1)} %param.14), kind=kOutput, calls=%fused_computation.58 | convolution fusion | flops 4296015872 | bytes 10485760 | tf_op jit(solution)/shard_map/dot_general | solution.py:33
  316.7 15.5 %bitcast_reduce_fusion = (f32[2,1024]{1,0:T(2,128)S(1)}, f32[2048,1024,2]{1,0,2:T(8,128)}) fusion(f32[2]{0:T(128)S(1)} %get-tuple-element.9, bf16[1024,2,512]{0,2,1:T(8,128)(2,1)S(1)} %bitcast.171, bf16[2048,2048]{1,0:T(8,128)(2,1)} %all-gather.6.cloned.1.call-done, f32[2048]{0:T(1024)S(1)} %bitcast.164, f32[2048]{0:T(1024)S(1)} %add_rsqrt_fusion, ...), kind=kOutput, calls=%fused_computation.8 | convolution fusion | flops 8616146944 | bytes 29384712 | tf_op jit(solution)/shard_map/thd,nd->htn/dot_general | solution.py:37
  332.2 8.6 %fusion.9 = f32[2,1024]{1,0:T(2,128)S(1)} fusion(f32[2048,1024,2]{1,0,2:T(8,128)} %get-tuple-element.14, f32[2,1024]{1,0:T(2,128)S(1)} %get-tuple-element.13, f32[2]{0:T(128)S(1)} %get-tuple-element.9), kind=kLoop, calls=%fused_computation.15 | loop fusion | flops 12580864 | bytes 16793608 | tf_op jit(solution)/shard_map/reduce_sum | solution.py:41
  340.8 11.9 %all-gather.1 = f32[8,2,1024]{2,1,0:T(2,128)S(1)} all-gather(f32[2,2,1024]{2,1,0:T(2,128)S(1)} %pad_maximum_fusion.1), channel_id=3, replica_groups=mesh['z'=4,'y'=4,'x'=4,'c'=2] {'z'}, dimensions={0}, use_global_device_ids=true | all-gather | bytes 81920 | tf_op jit(solution)/shard_map/all_gather | solution.py:43
  352.7 15.3 %fusion.21 = bf16[1024,2,512]{0,2,1:T(8,128)(2,1)S(1)} fusion(f32[2048,1024,2]{1,0,2:T(8,128)} %get-tuple-element.14, f32[2,1024]{1,0:T(2,128)S(1)} %get-tuple-element.13, f32[2]{0:T(128)S(1)} %get-tuple-element.9, bf16[2048,2048]{1,0:T(8,128)(2,1)} %all-gather.6.cloned.1.call-done, f32[2048]{0:T(1024)S(1)} %bitcast.165, f32[2048]{0:T(1024)S(1)} %add_rsqrt_fusion, ...), kind=kOutput, calls=%fused_computation.26 | convolution fusion | flops 8622440448 | bytes 29392904 | tf_op jit(solution)/shard_map/htn,nd->htd/dot_general | solution.py:42
  368.0 0.0 copy-start.2
  368.1 0.0 copy-start.1
  368.1 8.4 %fusion.36 = bf16[1024,2048]{1,0:T(8,128)(2,1)} fusion(bf16[1024,1024]{0,1:T(8,128)(2,1)S(1)} %bitcast.169, bf16[2,1024,2048]{2,1,0:T(8,128)(2,1)} %param.17), kind=kOutput, calls=%fused_computation.40 | convolution fusion | flops 4297064448 | bytes 10485760 | tf_op jit(solution)/shard_map/dot_general | solution.py:49
  376.4 0.0 reduce-scatter.5.cloned.1.call-update
  376.5 0.0 copy-done.2
  376.5 81.7 %reduce-scatter.5.cloned.1.call-done = bf16[32,2048]{1,0:T(8,128)(2,1)} async-done(((bf16[1024,2048]{1,0:T(8,128)(2,1)}), bf16[32,2048]{1,0:T(8,128)(2,1)}) %reduce-scatter.5.cloned.1.call-update) | async-done | bytes 131088 | tf_op jit(solution)/shard_map/reduce_scatter | solution.py:50
  458.2 0.0 copy-done.1
  458.2 1.1 multiply_reduce_fusion
  459.2 1.7 multiply_multiply_fusion
  (13 shorter events, 0.2 us)
Async XLA Ops:
  6.5 52.3 %all-gather.8.cloned.1.call-start = ((), (), s32[]{:S(2)}) async-start(), calls=%async_computation.3 | async-start | bytes 4325376 | tf_op jit(solution)/shard_map/all_gather | solution.py:32
  10.1 103.0 %all-gather.6.cloned.1.call-start = ((), (), s32[]{:S(2)}) async-start(), calls=%async_computation.2 | async-start | bytes 8650752 | tf_op jit(solution)/shard_map/all_gather | solution.py:24
  10.8 249.5 %reduce-scatter.3.cloned.1.call-start = ((), (), s32[]{:S(2)}) async-start(), calls=%async_computation.4 | async-start | bytes 4325376 | tf_op jit(solution)/shard_map/reduce_scatter | solution.py:50
  170.3 90.0 %copy-start = (bf16[32,2048]{1,0:T(8,128)(2,1)S(1)}, bf16[32,2048]{1,0:T(8,128)(2,1)}, u32[]{:S(2)}) copy-start(bf16[32,2048]{1,0:T(8,128)(2,1)} %param.10) | copy-start | bytes 393220
  178.7 129.9 %all-gather.10.cloned.1.call-start = ((), (), s32[]{:S(2)}) async-start(), calls=%async_computation.5 | async-start | bytes 4325376 | tf_op jit(solution)/shard_map/all_gather | solution.py:32
  263.0 195.1 %reduce-scatter.5.cloned.1.call-start = ((), (), s32[]{:S(2)}) async-start(), calls=%async_computation.6 | async-start | bytes 4325376 | tf_op jit(solution)/shard_map/reduce_scatter | solution.py:50
  368.0 8.4 %copy-start.2 = (bf16[2048]{0:T(1024)(128)(2,1)S(1)}, bf16[2048]{0:T(1024)(128)(2,1)}, u32[]{:S(2)}) copy-start(bf16[2048]{0:T(1024)(128)(2,1)} %param.19) | copy-start | bytes 12292
  368.1 90.1 %copy-start.1 = (bf16[32,2048]{1,0:T(8,128)(2,1)S(1)}, bf16[32,2048]{1,0:T(8,128)(2,1)}, u32[]{:S(2)}) copy-start(bf16[32,2048]{1,0:T(8,128)(2,1)} %reduce-scatter.3.cloned.1.call-done) | copy-start | bytes 393220
Sparse Core Ops, SparseCore 0:
  10.2 48.6 all-gather.7
  61.1 51.9 all-gather.5
  178.8 81.4 reduce-scatter.2
  263.1 45.4 all-gather.9
  376.6 81.5 reduce-scatter.4

commit v2 on v1

v2 whole, which is shorter than its diff:
```python
import functools
import math

import jax
import jax.numpy as jnp
from jax import lax
from jax.experimental import pallas as pl
from jax.experimental.pallas import tpu as pltpu
from jax.sharding import Mesh
from jax.sharding import PartitionSpec as P

HEAD_DIM = 512
D = 2048
EPS = 1e-06
ROWS = ("z", "y", "x", "c")
TP = ("x", "c")
MESH = pl.DeviceIdType.MESH
RING = 4
BF16 = jnp.bfloat16
F32 = jnp.float32
GROUPS = 4
SRC_PIECE = 16
TGT_PIECE = 16
VMEM_LIMIT = 64 * 1024 * 1024 - 64 * 1024
VIA = (1, -1, -1, 1)
AWAY = (0, 1, 2, 1)
XX = (("x", "z"),) * GROUPS
XZ = (("x", "z"), ("z", "x")) * 2
XY = (("x", "y"), ("y", "x")) * 2
ROUNDS = [
    sorted(
        [(i, j) for i in range(RING) for j in range(RING) if AWAY[i] + AWAY[j] == r],
        key=lambda p: (p[1] != 0, p),
    )
    for r in range(5)
]


def piece_no(h, i, j):
    return h * 16 + i * 4 + j


def source_slots():
    slots = {}
    for pairs in ROUNDS:
        for s in range(2):
            for h in range(GROUPS):
                for i, j in pairs:
                    slots[s, h, i, j] = len(slots)
    return slots


SRC_SLOT = source_slots()


def line_sends(h, o):
    if o == 0:
        return [(1, 3), (-1, 1)]
    if o == 1 and VIA[h] == 1:
        return [(-1, 2)]
    if o == 3 and VIA[h] == -1:
        return [(1, 2)]
    return []


def line_up(h, o):
    if o == 2:
        return (1, 1) if VIA[h] == 1 else (-1, 3)
    return (1, 0) if o == 1 else (-1, 0)


class Here:
    def __init__(self):
        self.at = {a: lax.axis_index(a) for a in ROWS}
        self.step = 1 - 2 * self.at["c"]

    def next(self, axis, k=1):
        return {axis: lax.rem(self.at[axis] + RING + k * self.step, RING)}

    def sibling(self):
        return {"c": 1 - self.at["c"]}


def greet(peers):
    barrier = pltpu.get_barrier_semaphore()
    for peer in peers:
        pl.semaphore_signal(barrier, inc=1, device_id=peer, device_id_type=MESH)
    pl.semaphore_wait(barrier, len(peers))


def start_all(copies):
    for copy in copies:
        copy.start()
    return copies


def wait_all(copies):
    for copy in copies:
        copy.wait()


class Gather:
    def __init__(self, here, ref, order, sems):
        self.here, self.ref, self.order = here, ref, order
        self.ring_send, self.ring_recv, self.sib_send, self.sib_recv = sems
        self.sent = []

    def ring(self, h, src, dst, axis, way):
        n = piece_no(h, *dst)
        return pltpu.make_async_remote_copy(
            self.ref(0, h, *src), self.ref(0, h, *dst), self.ring_send.at[n], self.ring_recv.at[n],
            device_id=self.here.next(axis, way), device_id_type=MESH,
        )

    def sib(self, h, i, j):
        n = piece_no(h, i, j)
        return pltpu.make_async_remote_copy(
            self.ref(0, h, i, j), self.ref(1, h, i, j), self.sib_send.at[n], self.sib_recv.at[n],
            device_id=self.here.sibling(), device_id_type=MESH,
        )

    def spread(self, h, i, j):
        copies = []
        first, second = self.order[h]
        if j == 0:
            copies += [self.ring(h, (i, 0), (o, 0), first, way) for way, o in line_sends(h, i)]
        copies += [self.ring(h, (i, j), (i, o), second, way) for way, o in line_sends(h, j)]
        copies.append(self.sib(h, i, j))
        self.sent += start_all(copies)

    def spread_own(self):
        for h in range(GROUPS):
            self.spread(h, 0, 0)

    def relay(self, r, h):
        for i, j in ROUNDS[r]:
            self.ring(h, (0, 0), (i, j), "x", 1).wait_recv()
            self.spread(h, i, j)

    def arrive_sib(self, r):
        for h in range(GROUPS):
            for i, j in ROUNDS[r]:
                self.sib(h, i, j).wait_recv()

    def finish(self):
        for copy in self.sent:
            copy.wait_send()
        self.sent = []


def source_ref(src):
    def ref(*piece):
        return src.at[pl.ds(SRC_SLOT[piece] * SRC_PIECE, SRC_PIECE), :]

    return ref


def place_of(order, h, i, j):
    return (j, i) if order[h][0] == "x" else (i, j)


def target_ref(tgt, order):
    def ref(s, h, i, j):
        zd, xd = place_of(order, h, i, j)
        row = ((zd * 2 + s) * 8 + (h % 2) * 4 + xd) * TGT_PIECE
        return tgt.at[pl.ds(row, TGT_PIECE), pl.ds((h // 2) * 1024, 1024)]

    return ref


def unit_times(values, gain):
    scale = lax.rsqrt(jnp.mean(values * values, axis=-1, keepdims=True) + EPS)
    return values * scale * gain.astype(F32)


def whole_kernel(
    target, source, target_gain, source_gain, head_temp, final_gain, query_w, key_w, value_w, out_w,
    result,
    src, tgt, kv_w, q_w, kv_buf, q_buf, g_buf,
    w_buf, e_buf, o_buf, p_buf, att, att_out, ring_out, ring_in, st_own, st_in, hidden,
    s_ring_send, s_ring_recv, s_sib_send, s_sib_recv,
    t_ring_send, t_ring_recv, t_sib_send, t_sib_recv,
    load_sem, st_send, st_recv, sib_send, sib_recv, ring_send, ring_recv,
):
    here = Here()

    def projection_loads(layer):
        return [
            pltpu.make_async_copy(key_w.at[layer], kv_w.at[:, 0:512], load_sem.at[0]),
            pltpu.make_async_copy(value_w.at[layer], kv_w.at[:, 512:1024], load_sem.at[1]),
            pltpu.make_async_copy(query_w.at[layer], q_w, load_sem.at[2]),
        ]

    def out_load(layer):
        return pltpu.make_async_copy(out_w.at[layer], w_buf.at[0:1024], load_sem.at[3])

    def out_share(layer):
        return pltpu.make_async_remote_copy(
            out_w.at[layer], w_buf.at[1024:2048], sib_send.at[4], sib_recv.at[4],
            device_id=here.sibling(), device_id_type=MESH,
        )

    def place_target(values, layer):
        normed = unit_times(values, target_gain[layer : layer + 1, :]).astype(BF16)
        for half in range(2):
            tgt[half * 64 : half * 64 + 16, :] = normed[half * 16 : half * 16 + 16]

    def project_kv(start, rows, part):
        def body(n, carry):
            cols = pl.ds(pl.multiple_of(part * 512 + n * 256, 256), 256)
            kv = jnp.dot(src[start : start + rows, :], kv_w[:, cols], preferred_element_type=F32)
            kv_buf[start : start + rows, cols] = kv.astype(BF16)
            return carry

        lax.fori_loop(0, 2, body, 0)

    def project_q(o):
        def body(n, carry):
            cols = pl.ds(pl.multiple_of(n * 512, 512), 512)
            rows = pl.ds(pl.multiple_of(n * 256, 256), 256)
            q = jnp.dot(tgt[o * 256 : o * 256 + 256, :], q_w[:, cols], preferred_element_type=F32)
            q_buf[o, rows, :] = q.astype(BF16)
            return carry

        lax.fori_loop(0, 2, body, 0)

    def spread_ratio():
        ratio = source_gain[1:2, :].astype(F32) / source_gain[0:1, :].astype(F32)
        for k in range(D // 128):
            at = slice(k * 128, k * 128 + 128)
            g_buf[at, :] = jnp.broadcast_to(ratio[:, at], (128, 128)).T

    def fold_ratio():
        def body(k, carry):
            rows = pl.ds(pl.multiple_of(k * 128, 128), 128)
            g = jnp.concatenate([g_buf[rows, :]] * 4, axis=1)
            for n in range(2):
                cols = pl.ds(n * 512, 512)
                kv_w[rows, cols] = (kv_w[rows, cols].astype(F32) * g).astype(BF16)
            return carry

        lax.fori_loop(0, D // 128, body, 0)

    weights = start_all(projection_loads(0))
    out_own = out_load(0)
    out_own.start()
    normed = unit_times(source[...].astype(F32), source_gain[0:1, :]).astype(BF16)
    for h in range(GROUPS):
        row = SRC_SLOT[0, h, 0, 0] * SRC_PIECE
        src[row : row + 16, :] = normed[h * 16 : h * 16 + 16]
    place_target(target[...].astype(F32), 0)
    greet(
        [here.next(a, k) for a in "xyz" for k in (1, -1)] + [here.next("z", 2), here.sibling()]
    )
    sg = Gather(here, source_ref(src), XY, (s_ring_send, s_ring_recv, s_sib_send, s_sib_recv))
    tg = Gather(here, target_ref(tgt, XX), XX, (t_ring_send, t_ring_recv, t_sib_send, t_sib_recv))
    sg.spread_own()
    tg.spread_own()
    out_sib = out_share(0)
    out_sib.start()
    spread_ratio()
    wait_all(weights)
    for r in range(1, 5):
        for h in range(GROUPS):
            tg.relay(r, h)
            sg.relay(r, h)
            if h == 0:
                sg.arrive_sib(r - 1)
                tg.arrive_sib(r - 1)
            if r == 2 and h % 2 == 1:
                project_kv(0, 640, h // 2)
            if r == 3 and h == 0:
                project_kv(640, 384, 0)
            if r == 3 and h == 1:
                project_kv(640, 384, 1)
            if r == 3 and h == 2:
                project_kv(1024, 384, 0)
            if r == 3 and h == 3:
                project_kv(1024, 384, 1)
            if r == 4 and h == 0:
                project_q(0)
    project_q(1)
    project_q(3)
    tg.arrive_sib(4)
    project_q(2)
    sg.arrive_sib(4)
    project_kv(1408, 640, 0)
    project_kv(1408, 640, 1)
    sg.finish()
    tg.finish()

    for layer in range(2):
        attention_layer(
            layer, here, head_temp, q_buf, kv_buf, w_buf, e_buf, o_buf, p_buf, att, att_out,
            ring_out, ring_in, st_own, st_in, st_send, st_recv, sib_send, sib_recv, ring_send, ring_recv,
            target if layer == 0 else hidden, result if layer else hidden,
            final_gain if layer else None,
            lambda: start_all(projection_loads(1)) if layer == 0 else [],
            (lambda loads: (wait_all(loads), fold_ratio())) if layer == 0 else (lambda loads: None),
            [functools.partial(project_kv, n * 512, 512, part) for n in range(2) for part in range(2)] if layer == 0 else [],
            out_own, out_sib,
        )
        if layer == 1:
            break
        out_sib.wait_send()
        place_target(hidden[...], 1)
        out_own = out_load(1)
        out_own.start()
        tg = Gather(here, target_ref(tgt, XZ), XZ, (t_ring_send, t_ring_recv, t_sib_send, t_sib_recv))
        tg.spread_own()
        for r in range(1, 5):
            for h in range(GROUPS):
                tg.relay(r, h)
            tg.arrive_sib(r - 1)
            if r == 1:
                out_sib = out_share(1)
                out_sib.start()
            if r < 4:
                project_kv(1024 + 512 * ((r - 1) // 2), 512, (r - 1) % 2)
            if r == 3:
                project_q(0)
        project_kv(1536, 512, 1)
        project_q(1)
        project_q(3)
        tg.arrive_sib(4)
        project_q(2)
        tg.finish()
    out_sib.wait_send()


PAIR = {2: (0, 0), 1: (0, 1), 3: (1, 0), 0: (1, 1)}


def attention_layer(
    layer, here, head_temp, q_buf, kv_buf, w_buf, e_buf, o_buf, p_buf, att, att_out,
    ring_out, ring_in, st_own, st_in, st_send, st_recv, sib_send, sib_recv, ring_send, ring_recv,
    before, after, final_gain, start_loads, use_loads, fillers, out_own, out_sib,
):
    pending = []
    loads = start_loads()
    log2e = 1.0 / math.log(2.0)
    upper = lax.broadcasted_iota(jnp.int32, (512, 1), 0) < 256
    scale = jnp.where(upper, head_temp[layer, 0], head_temp[layer, 1]) * (HEAD_DIM ** (-0.5) * log2e)

    def stats_copy(k):
        return pltpu.make_async_remote_copy(
            st_own, st_in.at[k - 1], st_send.at[k - 1], st_recv.at[k - 1],
            device_id=here.next("z", k), device_id_type=MESH,
        )

    def score(o, carry):
        scores = lax.dot_general(
            q_buf[o], kv_buf[:, 0:512], (((1,), (1,)), ((), ())), preferred_element_type=F32
        )
        top = jnp.max(scores, axis=-1, keepdims=True)
        expo = jnp.exp2((scores - top) * scale)
        total = jnp.sum(expo, axis=-1, keepdims=True)
        e_buf[o] = expo.astype(BF16)
        lane = lax.broadcasted_iota(jnp.int32, (512, 128), 1)
        both = jnp.where(lane == 0, top * scale, total)
        st_own[o] = both.T[0:8, :]
        return carry

    def attend(o):
        return jnp.dot(e_buf[o], kv_buf[:, 512:1024], preferred_element_type=F32)

    def att_copy(o):
        pair, at = PAIR[o]
        return pltpu.make_async_remote_copy(
            att_out.at[o], att.at[pair, at * 128 : at * 128 + 128, 1024:2048], sib_send.at[o], sib_recv.at[o],
            device_id=here.sibling(), device_id_type=MESH,
        )

    def peer_stats(k, o, what):
        parts = []
        for n in range(4):
            there = (o + k) % RING if n % 2 == 0 else (o - k) % RING
            parts.append(st_in[k - 1, there, what : what + 1, n * 128 : n * 128 + 128])
        return jnp.concatenate(parts, axis=1)

    def weigh(o, values):
        own = st_own[o]
        tops = [own[0:1]] + [peer_stats(k, o, 0) for k in range(1, RING)]
        totals = [own[1:2]] + [peer_stats(k, o, 1) for k in range(1, RING)]
        top = functools.reduce(jnp.maximum, tops)
        total = sum(t * jnp.exp2(m - top) for m, t in zip(tops, totals))
        factor = jnp.exp2(own[0:1] - top) / total
        factor = jnp.broadcast_to(factor, (128, 512)).T
        factor = jnp.concatenate([factor] * 4, axis=1)
        rows = (values * factor).astype(BF16)
        pair, at = PAIR[o]
        for head in range(2):
            cols = slice(head * 512, head * 512 + 512)
            att_out[o, :, cols] = rows[head * 256 + 128 : head * 256 + 256]
            att[pair, at * 128 : at * 128 + 128, cols] = rows[head * 256 : head * 256 + 128]
        pending.extend(start_all([att_copy(o)]))

    def mix(pair):
        def body(n, carry):
            cols = pl.ds(pl.multiple_of(n * 512, 512), 512)
            p_buf[pair, :, cols] = jnp.dot(att[pair], w_buf[:, cols], preferred_element_type=F32)
            return carry

        lax.fori_loop(0, 4, body, 0)

    def ring_copy(h, i, j):
        axis, way = (XZ[h][1], line_up(h, j)[0]) if j else (XZ[h][0], line_up(h, i)[0])
        n = piece_no(h, i, j)
        return pltpu.make_async_remote_copy(
            ring_out.at[n], ring_in.at[n], ring_send.at[n], ring_recv.at[n],
            device_id=here.next(axis, way), device_id_type=MESH,
        )

    def below(h, i, j):
        labels = [(i, o) for way, o in line_sends(h, j)]
        if j == 0:
            labels += [(o, 0) for way, o in line_sends(h, i)]
        return labels

    def collect(h, i, j):
        zd, xd = place_of(XZ, h, i, j)
        pair, at = PAIR[zd]
        rows = pl.ds(at * 128 + ((h % 2) * 4 + xd) * 16, 16)
        value = p_buf[pair, rows, pl.ds((h // 2) * 1024, 1024)]
        for label in below(h, i, j):
            ring_copy(h, *label).wait_recv()
            value += ring_in[piece_no(h, *label)].astype(F32)
        return value

    def pass_on(h, i, j):
        ring_out[piece_no(h, i, j)] = collect(h, i, j).astype(BF16)
        pending.extend(start_all([ring_copy(h, i, j)]))

    passed = set()

    def pass_leaves(pair):
        for r in (4, 3, 2, 1):
            for h in range(GROUPS):
                for label in ROUNDS[r]:
                    zd, _ = place_of(XZ, h, *label)
                    if PAIR[zd][0] == pair and not below(h, *label):
                        pass_on(h, *label)
                        passed.add((h, label))

    lax.fori_loop(0, 4, score, 0)
    for k in range(1, RING):
        pending.extend(start_all([stats_copy(k)]))
    o_buf[0] = attend(2)
    o_buf[1] = attend(1)
    use_loads(loads)
    for k in range(1, RING):
        stats_copy(k).wait_recv()
    weigh(2, o_buf[0])
    weigh(1, o_buf[1])
    weigh(3, attend(3))
    weigh(0, attend(0))
    out_own.wait()
    out_sib.wait_recv()
    att_copy(2).wait_recv()
    att_copy(1).wait_recv()
    mix(0)
    pass_leaves(0)
    att_copy(3).wait_recv()
    att_copy(0).wait_recv()
    mix(1)
    pass_leaves(1)
    fillers = list(fillers)
    for r in (3, 2, 1):
        if fillers:
            fillers.pop(0)()
        for h in range(GROUPS):
            for label in ROUNDS[r]:
                if (h, label) not in passed:
                    pass_on(h, *label)
    for filler in fillers:
        filler()
    for half in range(2):
        at = slice(half * 16, half * 16 + 16)
        value = jnp.concatenate([collect(half, 0, 0), collect(half + 2, 0, 0)], axis=1)
        value += before[at, :].astype(F32)
        if final_gain is not None:
            value = unit_times(value, final_gain[...])
        after[at, :] = value
    for copy in pending:
        copy.wait_send()


def vmem(*shape, dtype=BF16):
    return pltpu.VMEM(shape, dtype)


ANY = pl.BlockSpec(memory_space=pl.ANY)
INV = pl.BlockSpec(memory_space=pltpu.VMEM)
DMA = pltpu.SemaphoreType.DMA


def per_device(
    target, source, target_gain, source_gain, query_w, key_w, value_w, out_w, head_temp, final_gain
):
    return pl.pallas_call(
        whole_kernel,
        out_shape=jax.ShapeDtypeStruct((32, D), F32),
        in_specs=[INV, INV, INV, INV, pl.BlockSpec(memory_space=pltpu.SMEM), INV, ANY, ANY, ANY, ANY],
        out_specs=INV,
        scratch_shapes=[
            vmem(2048, D), vmem(1024, D), vmem(D, 1024), vmem(D, 1024), vmem(2048, 1024), vmem(4, 512, HEAD_DIM),
            vmem(D, 128, dtype=F32),
            vmem(2048, D), vmem(4, 512, 2048), vmem(2, 512, HEAD_DIM, dtype=F32), vmem(2, 256, D, dtype=F32),
            vmem(2, 256, D), vmem(4, 128, 1024), vmem(64, 16, 1024), vmem(64, 16, 1024),
            vmem(4, 8, 512, dtype=F32), vmem(3, 4, 8, 512, dtype=F32), vmem(32, D, dtype=F32),
        ] + [DMA((64,))] * 8 + [DMA((4,)), DMA((3,)), DMA((3,)), DMA((5,)), DMA((5,)), DMA((64,)), DMA((64,))],
        compiler_params=pltpu.CompilerParams(
            collective_id=0, has_side_effects=True, vmem_limit_bytes=VMEM_LIMIT
        ),
        name="whole",
    )(target, source, target_gain, source_gain, head_temp, final_gain.reshape(1, D), query_w, key_w, value_w, out_w)


def solution(mesh):
    split = Mesh(mesh.devices.reshape(4, 4, 4, 2), ROWS)
    in_specs = (
        P(ROWS, None),
        P(ROWS, None),
        P(),
        P(),
        P(None, None, TP),
        P(None, None, TP),
        P(None, None, TP),
        P(None, TP, None),
        P(None, TP),
        P(),
    )
    return jax.shard_map(
        per_device, mesh=split, in_specs=in_specs, out_specs=P(ROWS, None), check_vma=False
    )
```

time: 473 us -> 152 us (0.32)
  waiting for transfers between devices: 302 us -> 0 us
  Pallas kernels: 0 us -> 148 us
  matrix products: 94.7 us -> 0 us
  other arithmetic: 33 us -> 0 us
  blocking collectives: 24.2 us -> 0 us
  between operations: 13.5 us -> 0.01 us
    reduce_scatter x2 -> x0, waiting for transfers between devices: 163 us -> none  [per_device(): mixed = lax.psum_scatter(part, TGT_PLANE, scatter_dimension=0, tiled=True)]
    pallas_call x0 -> x1, Pallas kernels: none -> 148 us  [per_device(): pl.pallas_call(whole_kernel, out_shape=jax.ShapeDtypeStruct((32, D), F32)...]
    all_gather x3 -> x0, waiting for transfers between devices: 138 us -> none  [the longest x2 92 us: per_device(): full = lax.all_gather(normed, TGT_PLANE, axis=0, tiled=True)]
    dot_general x8 -> x0, matrix products: 94.7 us -> none  [the longest x2 31.3 us: per_device(): s = jnp.einsum('thd,nd->htn', q, k, preferred_element_type=jnp.float32)]
    reduce_sum x8 -> x0, other arithmetic: 25.4 us -> none  [the longest x2 17.1 us: per_device(): t = jnp.sum(e, axis=-1)]
    all_gather x2 -> x0, blocking collectives: 24.2 us -> none  [per_device(): stats = lax.all_gather(jnp.stack([m, t]), 'z')]
  transfers between devices with their start and end apart: 5 -> 0, of which waited for: 5 -> 0; matrix products, arithmetic and copies ran while one was open for 2% -> 0% of each run, Pallas kernels for 0% -> 0%
where the time goes in v2:
time: 152 us; the launch traced here: 151 us
  Pallas kernels  148 us (97%)
  local copies, waits for them, and re-layouts  2.96 us (2%)
    pallas_call x1, Pallas kernels, per_device(): pl.pallas_call(whole_kernel, out_shape=jax.ShapeDtypeStruct((32, D), F32)...  148 us

profile of v2, /device:TPU:0, one launch (start us, length us, event | category | flops | bytes accessed | tf_op | source)
XLA Modules:
  0.0 151.4 jit_solution(15937000131403614579)
XLA Ops:
  0.0 1.3 reshape.3.final_gain
  1.3 148.4 %whole.1 = f32[32,2048]{1,0:T(8,128)} custom-call(bf16[32,2048]{1,0:T(8,128)(2,1)} %target.1, bf16[64,2048]{1,0:T(8,128)(2,1)} %source.1, bf16[2,2048]{1,0:T(2,128)(2,1)} %target_gain.1, bf16[2,2048]{1,0:T(2,128)(2,1)} %source_gain.1, f32[2,2]{1,0:T(2,128)} %head_temp.1, bf16[1,2048]{1,0:T(2,128)(2,1)} %reshape.3.final_gain, bf16[2,2048,1024]{2,1,0:T(8,128)(2,1)} %query_w.1, ...), custom_call_target="tpu_custom_call" | custom-call | tf_op jit(solution)/shard_map/whole/pallas_call | solution.py:500
  149.7 1.7 %copy.12 = f32[32,2048]{1,0:T(8,128)} copy(f32[32,2048]{1,0:T(8,128)} %whole.1) | data formatting | bytes 524288

commit v3 on v1

v3 whole, which is shorter than its diff:
```python
import functools
import math

import jax
import jax.numpy as jnp
from jax import lax
from jax.experimental import pallas as pl
from jax.experimental.pallas import tpu as pltpu
from jax.sharding import Mesh
from jax.sharding import PartitionSpec as P

HEAD_DIM = 512
D = 2048
EPS = 1e-06
ROWS = ("z", "y", "x", "c")
TP = ("x", "c")
MESH = pl.DeviceIdType.MESH
RING = 4
BF16 = jnp.bfloat16
F32 = jnp.float32
GROUPS = 4
SRC_PIECE = 16
TGT_PIECE = 16
VMEM_LIMIT = 64 * 1024 * 1024 - 64 * 1024
VIA = (1, -1, -1, 1)
AWAY = (0, 1, 2, 1)
XX = (("x", "z"),) * GROUPS
XZ = (("x", "z"), ("z", "x")) * 2
XY = (("x", "y"), ("y", "x")) * 2
ROUNDS = [
    sorted(
        [(i, j) for i in range(RING) for j in range(RING) if AWAY[i] + AWAY[j] == r],
        key=lambda p: (p[1] != 0, p),
    )
    for r in range(5)
]


POS = {2: 0, 1: 1, 3: 2, 0: 3}


def piece_no(h, i, j):
    return h * 16 + i * 4 + j


def source_slots():
    slots = {}
    for pairs in ROUNDS:
        for s in range(2):
            for h in range(GROUPS):
                for i, j in pairs:
                    slots[s, h, i, j] = len(slots)
    return slots


SRC_SLOT = source_slots()


def line_sends(h, o):
    if o == 0:
        return [(1, 3), (-1, 1)]
    if o == 1 and VIA[h] == 1:
        return [(-1, 2)]
    if o == 3 and VIA[h] == -1:
        return [(1, 2)]
    return []


def line_up(h, o):
    if o == 2:
        return (1, 1) if VIA[h] == 1 else (-1, 3)
    return (1, 0) if o == 1 else (-1, 0)


def below(h, i, j):
    labels = [(i, o) for way, o in line_sends(h, j)]
    if j == 0:
        labels += [(o, 0) for way, o in line_sends(h, i)]
    return labels


JOINS = [
    (h, i, j) for h in range(GROUPS) for i in range(RING) for j in range(RING) if below(h, i, j)
]


class Here:
    def __init__(self):
        self.at = {a: lax.axis_index(a) for a in ROWS}
        self.step = 1 - 2 * self.at["c"]

    def next(self, axis, k=1):
        return {axis: lax.rem(self.at[axis] + RING + k * self.step, RING)}

    def sibling(self):
        return {"c": 1 - self.at["c"]}


def greet(peers):
    barrier = pltpu.get_barrier_semaphore()
    for peer in peers:
        pl.semaphore_signal(barrier, inc=1, device_id=peer, device_id_type=MESH)
    pl.semaphore_wait(barrier, len(peers))


def start_all(copies):
    for copy in copies:
        copy.start()
    return copies


def wait_all(copies):
    for copy in copies:
        copy.wait()


class Gather:
    def __init__(self, here, ref, bulk, order, sems, groups=tuple(range(GROUPS)), tag=0):
        self.here, self.ref, self.bulk, self.order = here, ref, bulk, order
        send, self.ring_recv, self.sib_recv = sems
        self.groups, self.tag, self.send = groups, tag, send.at[tag]
        self.sent = 0

    def ring(self, h, src, dst, axis, way):
        r = AWAY[dst[0]] + AWAY[dst[1]]
        return pltpu.make_async_remote_copy(
            self.ref(0, h, *src), self.ref(0, h, *dst), self.send, self.ring_recv.at[(r - 1) * GROUPS + h],
            device_id=self.here.next(axis, way), device_id_type=MESH,
        )

    def sib(self, h, i, j):
        return pltpu.make_async_remote_copy(
            self.ref(0, h, i, j), self.ref(1, h, i, j), self.send, self.sib_recv.at[self.tag * 5 + AWAY[i] + AWAY[j]],
            device_id=self.here.sibling(), device_id_type=MESH,
        )

    def whole(self, n, recv):
        return pltpu.make_async_remote_copy(
            self.bulk(n), self.bulk(n), self.send, recv,
            device_id=self.here.sibling(), device_id_type=MESH,
        )

    def spread(self, h, i, j):
        copies = []
        first, second = self.order[h]
        if j == 0:
            copies += [self.ring(h, (i, 0), (o, 0), first, way) for way, o in line_sends(h, i)]
        copies += [self.ring(h, (i, j), (i, o), second, way) for way, o in line_sends(h, j)]
        copies.append(self.sib(h, i, j))
        self.sent += len(start_all(copies))

    def spread_own(self):
        for h in self.groups:
            self.spread(h, 0, 0)

    def relay(self, r, h):
        self.whole(len(ROUNDS[r]), self.ring_recv.at[(r - 1) * GROUPS + h]).wait_recv()
        for i, j in ROUNDS[r]:
            self.spread(h, i, j)

    def arrive_sib(self, r):
        self.whole(len(ROUNDS[r]) * len(self.groups), self.sib_recv.at[self.tag * 5 + r]).wait_recv()

    def finish(self):
        self.whole(self.sent, self.sib_recv.at[0]).wait_send()
        self.sent = 0


def source_ref(src):
    def ref(*piece):
        return src.at[pl.ds(SRC_SLOT[piece] * SRC_PIECE, SRC_PIECE), :]

    return ref


def source_bulk(src):
    return lambda n: src.at[pl.ds(0, n * SRC_PIECE), :]


def place_of(order, h, i, j):
    return (j, i) if order[h][0] == "x" else (i, j)


def target_ref(tgt, order):
    def ref(s, h, i, j):
        zd, xd = place_of(order, h, i, j)
        row = (h % 2) * 512 + POS[zd] * 128 + s * 64 + xd * TGT_PIECE
        return tgt.at[pl.ds(row, TGT_PIECE), pl.ds((h // 2) * 1024, 1024)]

    return ref


def target_bulk(tgt):
    def bulk(n):
        if n <= 64:
            return tgt.at[pl.ds(0, n * TGT_PIECE), pl.ds(0, 1024)]
        return tgt.at[pl.ds(0, n * TGT_PIECE // 2), :]

    return bulk


def unit_times(values, gain):
    scale = lax.rsqrt(jnp.mean(values * values, axis=-1, keepdims=True) + EPS)
    return values * scale * gain.astype(F32)


def whole_kernel(
    target, source, target_gain, source_gain, head_temp, final_gain, query_w, key_w, value_w, out_w,
    result,
    src, tgt, kv_w, q_w, kv_buf, q_buf, g_buf,
    w_buf, e_buf, p_buf, att, att_out, ring_out, ring_in, st_own, st_in, hidden,
    s_send, s_ring_recv, s_sib_recv, t_send, t_ring_recv, t_sib_recv,
    load_sem, st_send, st_recv, sib_send, sib_recv, ring_send, ring_recv,
):
    here = Here()

    def projection_loads(layer):
        return [
            pltpu.make_async_copy(key_w.at[layer], kv_w.at[:, 0:512], load_sem.at[0]),
            pltpu.make_async_copy(value_w.at[layer], kv_w.at[:, 512:1024], load_sem.at[1]),
            pltpu.make_async_copy(query_w.at[layer], q_w, load_sem.at[2]),
        ]

    def out_load(layer):
        return pltpu.make_async_copy(out_w.at[layer], w_buf.at[0:1024], load_sem.at[3])

    def out_share(layer):
        return pltpu.make_async_remote_copy(
            out_w.at[layer], w_buf.at[1024:2048], sib_send.at[2], sib_recv.at[2],
            device_id=here.sibling(), device_id_type=MESH,
        )

    def place_target(values, layer, half):
        normed = unit_times(values, target_gain[layer : layer + 1, :]).astype(BF16)
        row = half * 512 + POS[0] * 128
        tgt[row : row + 16, :] = normed

    def project_kv(layer, start, rows, part):
        def body(n, carry):
            cols = pl.ds(pl.multiple_of(part * 512 + n * 256, 256), 256)
            kv = jnp.dot(src[start : start + rows, :], kv_w[:, cols], preferred_element_type=F32)
            kv_buf[layer, start : start + rows, cols] = kv.astype(BF16)
            return carry

        lax.fori_loop(0, 2, body, 0)

    def project_q(half, pair):
        start = half * 512 + pair * 256
        def body(head, carry):
            cols = pl.ds(pl.multiple_of(head * 512, 512), 512)
            q = jnp.dot(tgt[start : start + 256, :], q_w[:, cols], preferred_element_type=F32).astype(BF16)
            for n in range(4):
                rows = pl.ds(pl.multiple_of(n * 128 + head * 64, 64), 64)
                q_buf[half, pair, rows, :] = q[n * 64 : n * 64 + 64]
            return carry

        lax.fori_loop(0, 2, body, 0)

    def spread_ratio():
        ratio = source_gain[1:2, :].astype(F32) / source_gain[0:1, :].astype(F32)
        for k in range(D // 128):
            at = slice(k * 128, k * 128 + 128)
            g_buf[at, :] = jnp.broadcast_to(ratio[:, at], (128, 128)).T

    def fold_ratio():
        def body(k, carry):
            rows = pl.ds(pl.multiple_of(k * 128, 128), 128)
            g = jnp.concatenate([g_buf[rows, :]] * 4, axis=1)
            for n in range(2):
                cols = pl.ds(n * 512, 512)
                kv_w[rows, cols] = (kv_w[rows, cols].astype(F32) * g).astype(BF16)
            return carry

        lax.fori_loop(0, D // 128, body, 0)

    log2e = 1.0 / math.log(2.0)
    first_head = lax.rem(lax.broadcasted_iota(jnp.int32, (512, 1), 0), 128) < 64
    pending = ([], [])

    def stats_copy(half, k):
        return pltpu.make_async_remote_copy(
            st_own.at[half], st_in.at[k - 1, half], st_send.at[k - 1, half], st_recv.at[k - 1, half],
            device_id=here.next("z", k), device_id_type=MESH,
        )

    def score(layer, half, pair):
        scale = jnp.where(first_head, head_temp[layer, 0], head_temp[layer, 1]) * (HEAD_DIM ** (-0.5) * log2e)
        scores = lax.dot_general(
            q_buf[half, pair], kv_buf[layer, :, 0:512], (((1,), (1,)), ((), ())), preferred_element_type=F32
        )
        top = jnp.max(scores, axis=-1, keepdims=True)
        expo = jnp.exp2((scores - top) * scale)
        total = jnp.sum(expo, axis=-1, keepdims=True)
        e_buf[pair] = expo.astype(BF16)
        lane = lax.broadcasted_iota(jnp.int32, (512, 128), 1)
        both = jnp.where(lane == 0, top * scale, total)
        st_own[half, pair] = both.T[0:8, :]

    def send_stats(half):
        for k in range(1, RING):
            pending[half].extend(start_all([stats_copy(half, k)]))

    def wait_stats(half):
        for k in range(1, RING):
            stats_copy(half, k).wait_recv()

    def att_copy(half):
        return pltpu.make_async_remote_copy(
            att_out.at[half], att.at[half, :, 1024:2048], sib_send.at[half], sib_recv.at[half],
            device_id=here.sibling(), device_id_type=MESH,
        )

    def peer_stats(k, half, pair, what):
        parts = []
        for n in range(4):
            zd = ((2, 1), (3, 0))[pair][n // 2]
            at = POS[(zd + k) % RING if n % 2 == 0 else (zd - k) % RING]
            lanes = (at % 2) * 256 + (n % 2) * 128
            parts.append(st_in[k - 1, half, at // 2, what : what + 1, lanes : lanes + 128])
        return jnp.concatenate(parts, axis=1)

    def weigh(layer, half, pair):
        own = st_own[half, pair]
        tops = [own[0:1]] + [peer_stats(k, half, pair, 0) for k in range(1, RING)]
        totals = [own[1:2]] + [peer_stats(k, half, pair, 1) for k in range(1, RING)]
        top = functools.reduce(jnp.maximum, tops)
        total = sum(t * jnp.exp2(m - top) for m, t in zip(tops, totals))
        factor = jnp.exp2(own[0:1] - top) / total
        factor = jnp.broadcast_to(factor, (128, 512)).T
        factor = jnp.concatenate([factor] * 4, axis=1)
        values = jnp.dot(e_buf[pair], kv_buf[layer, :, 512:1024], preferred_element_type=F32)
        rows = (values * factor).astype(BF16)
        for n in range(4):
            at = slice((pair * 2 + n // 2) * 64, (pair * 2 + n // 2) * 64 + 64)
            for head in range(2):
                cols = slice(head * 512, head * 512 + 512)
                part = rows[n * 128 + head * 64 : n * 128 + head * 64 + 64]
                if n % 2 == 0:
                    att[half, at, cols] = part
                else:
                    att_out[half, at, cols] = part

    def send_att(half):
        pending[half].extend(start_all([att_copy(half)]))

    def mix(half):
        att_copy(half).wait_recv()

        def body(n, carry):
            cols = pl.ds(pl.multiple_of(n * 512, 512), 512)
            p_buf[half, :, cols] = jnp.dot(att[half], w_buf[:, cols], preferred_element_type=F32)
            return carry

        lax.fori_loop(0, 4, body, 0)

    def ring_copy(h, i, j):
        if j:
            way, up = line_up(h, j)
            axis, parent = XZ[h][1], (i, up)
        else:
            way, up = line_up(h, i)
            axis, parent = XZ[h][0], (up, 0)
        n = piece_no(h, i, j)
        return pltpu.make_async_remote_copy(
            ring_out.at[n], ring_in.at[n], ring_send.at[h % 2], ring_recv.at[JOINS.index((h, *parent))],
            device_id=here.next(axis, way), device_id_type=MESH,
        )

    def ring_bulk(half, n, recv):
        return pltpu.make_async_remote_copy(
            ring_out.at[0:n], ring_in.at[0:n], ring_send.at[half], recv,
            device_id=here.sibling(), device_id_type=MESH,
        )

    def collect(h, i, j):
        zd, xd = place_of(XZ, h, i, j)
        rows = pl.ds(POS[zd] * 64 + xd * 16, 16)
        value = p_buf[h % 2, rows, pl.ds((h // 2) * 1024, 1024)]
        labels = below(h, i, j)
        if labels:
            ring_bulk(h % 2, len(labels), ring_recv.at[JOINS.index((h, i, j))]).wait_recv()
        for label in labels:
            value += ring_in[piece_no(h, *label)].astype(F32)
        return value

    def pass_on(h, i, j):
        ring_out[piece_no(h, i, j)] = collect(h, i, j).astype(BF16)
        ring_copy(h, i, j).start()

    def reduce_leaves(half):
        for r in (4, 3, 2, 1):
            for h in (half, half + 2):
                for label in ROUNDS[r]:
                    if not below(h, *label):
                        pass_on(h, *label)

    def reduce_round(half, r):
        for h in (half, half + 2):
            for label in ROUNDS[r]:
                if below(h, *label):
                    pass_on(h, *label)

    def reduce_end(layer, half):
        at = slice(half * 16, half * 16 + 16)
        value = jnp.concatenate([collect(half, 0, 0), collect(half + 2, 0, 0)], axis=1)
        value += (hidden if layer else target)[at, :].astype(F32)
        ring_bulk(half, 30, ring_recv.at[0]).wait_send()
        for copy in pending[half]:
            copy.wait_send()
        pending[half].clear()
        if layer:
            result[at, :] = unit_times(value, final_gain[...][None, :])
        else:
            hidden[at, :] = value
            place_target(value, 1, half)

    def target_gathers(order):
        return [
            Gather(
                here, target_ref(tgt, order), target_bulk(tgt), order,
                (t_send, t_ring_recv, t_sib_recv), (half, half + 2), half,
            )
            for half in range(2)
        ]

    weights = start_all(projection_loads(0))
    out_own = out_load(0)
    out_own.start()
    normed = unit_times(source[...].astype(F32), source_gain[0:1, :]).astype(BF16)
    for h in range(GROUPS):
        row = SRC_SLOT[0, h, 0, 0] * SRC_PIECE
        src[row : row + 16, :] = normed[h * 16 : h * 16 + 16]
    for half in range(2):
        place_target(target[half * 16 : half * 16 + 16, :].astype(F32), 0, half)
    greet(
        [here.next(a, k) for a in "xyz" for k in (1, -1)] + [here.next("z", 2), here.sibling()]
    )
    sg = Gather(here, source_ref(src), source_bulk(src), XY, (s_send, s_ring_recv, s_sib_recv))
    tg = target_gathers(XX)
    sg.spread_own()
    for g in tg:
        g.spread_own()
    out_sib = out_share(0)
    out_sib.start()
    spread_ratio()
    wait_all(weights)
    for h in range(GROUPS):
        tg[h % 2].relay(1, h)
    for r in range(1, 5):
        for h in range(GROUPS):
            if r < 4:
                tg[h % 2].relay(r + 1, h)
            if r < 4 or h == 0:
                sg.relay(r, h)
            if h == 0:
                sg.arrive_sib(r - 1)
                for g in tg:
                    g.arrive_sib(r - 1)
            if r == 2 and h % 2 == 1:
                project_kv(0, 0, 640, h // 2)
            if r == 3:
                project_kv(0, 640 + 384 * (h // 2), 384, h % 2)
            if r == 4 and h == 0:
                project_q(0, 1)
    project_q(1, 1)
    for half in range(2):
        tg[half].arrive_sib(4)
        project_q(half, 0)
    for h in range(1, GROUPS):
        sg.relay(4, h)
    sg.arrive_sib(4)
    project_kv(0, 1408, 640, 0)
    project_kv(0, 1408, 640, 1)
    sg.finish()
    for g in tg:
        g.finish()

    loads = start_all(projection_loads(1))
    tg = target_gathers(XZ)
    blocks = [(start, part) for start in range(0, 2048, 512) for part in range(2)]

    def fill(n=1):
        for _ in range(n):
            start, part = blocks.pop(0)
            project_kv(1, start, 512, part)

    def score_pair(pair, carry):
        score(0, 0, pair)
        return carry

    lax.fori_loop(0, 2, score_pair, 0)
    send_stats(0)
    wait_all(loads)
    fold_ratio()
    wait_stats(0)
    weigh(0, 0, 0)
    weigh(0, 0, 1)
    send_att(0)
    out_own.wait()
    out_sib.wait()
    fill(2)
    mix(0)
    reduce_leaves(0)
    score(0, 1, 0)
    reduce_round(0, 3)
    score(0, 1, 1)
    send_stats(1)
    reduce_round(0, 2)
    fill()
    reduce_round(0, 1)
    wait_stats(1)
    weigh(0, 1, 0)
    reduce_end(0, 0)
    tg[0].spread_own()
    weigh(0, 1, 1)
    send_att(1)
    fill()
    relay = lambda half, r: [tg[half].relay(r, h) for h in (half, half + 2)]
    relay(0, 1)
    mix(1)
    reduce_leaves(1)
    out_own = out_load(1)
    out_own.start()
    relay(0, 2)
    fill()
    reduce_round(1, 3)
    relay(0, 3)
    fill()
    reduce_round(1, 2)
    relay(0, 4)
    fill()
    reduce_round(1, 1)
    for r in range(4):
        tg[0].arrive_sib(r)
    project_q(0, 1)
    reduce_end(0, 1)
    tg[1].spread_own()
    tg[0].arrive_sib(4)
    project_q(0, 0)
    relay(1, 1)
    fill()
    tg[1].arrive_sib(0)
    out_sib = out_share(1)
    out_sib.start()
    score(1, 0, 0)
    relay(1, 2)
    score(1, 0, 1)
    send_stats(0)
    relay(1, 3)
    tg[1].arrive_sib(1)
    tg[1].arrive_sib(2)
    relay(1, 4)
    tg[1].arrive_sib(3)
    project_q(1, 1)
    wait_stats(0)
    weigh(1, 0, 0)
    weigh(1, 0, 1)
    send_att(0)
    tg[1].arrive_sib(4)
    project_q(1, 0)
    out_own.wait()
    out_sib.wait()
    mix(0)
    reduce_leaves(0)
    score(1, 1, 0)
    reduce_round(0, 3)
    score(1, 1, 1)
    send_stats(1)
    reduce_round(0, 2)
    reduce_round(0, 1)
    wait_stats(1)
    weigh(1, 1, 0)
    weigh(1, 1, 1)
    send_att(1)
    reduce_end(1, 0)
    mix(1)
    reduce_leaves(1)
    for r in (3, 2, 1):
        reduce_round(1, r)
    reduce_end(1, 1)
    for g in tg:
        g.finish()


def vmem(*shape, dtype=BF16):
    return pltpu.VMEM(shape, dtype)


ANY = pl.BlockSpec(memory_space=pl.ANY)
INV = pl.BlockSpec(memory_space=pltpu.VMEM)
DMA = pltpu.SemaphoreType.DMA


def per_device(
    target, source, target_gain, source_gain, query_w, key_w, value_w, out_w, head_temp, final_gain
):
    return pl.pallas_call(
        whole_kernel,
        out_shape=jax.ShapeDtypeStruct((32, D), F32),
        in_specs=[INV, INV, INV, INV, pl.BlockSpec(memory_space=pltpu.SMEM), INV, ANY, ANY, ANY, ANY],
        out_specs=INV,
        scratch_shapes=[
            vmem(2048, D), vmem(1024, D), vmem(D, 1024), vmem(D, 1024), vmem(2, 2048, 1024),
            vmem(2, 2, 512, HEAD_DIM), vmem(D, 128, dtype=F32),
            vmem(2048, D), vmem(2, 512, 2048), vmem(2, 256, D, dtype=F32),
            vmem(2, 256, D), vmem(2, 256, 1024), vmem(64, 16, 1024), vmem(64, 16, 1024),
            vmem(2, 2, 8, 512, dtype=F32), vmem(3, 2, 2, 8, 512, dtype=F32), vmem(32, D, dtype=F32),
            DMA((1,)), DMA((16,)), DMA((5,)), DMA((2,)), DMA((16,)), DMA((10,)),
            DMA((4,)), DMA((3, 2)), DMA((3, 2)), DMA((3,)), DMA((3,)), DMA((2,)), DMA((len(JOINS),)),
        ],
        compiler_params=pltpu.CompilerParams(
            collective_id=0, has_side_effects=True, vmem_limit_bytes=VMEM_LIMIT
        ),
        name="whole",
    )(target, source, target_gain, source_gain, head_temp, final_gain, query_w, key_w, value_w, out_w)


def solution(mesh):
    split = Mesh(mesh.devices.reshape(4, 4, 4, 2), ROWS)
    in_specs = (
        P(ROWS, None),
        P(ROWS, None),
        P(),
        P(),
        P(None, None, TP),
        P(None, None, TP),
        P(None, None, TP),
        P(None, TP, None),
        P(None, TP),
        P(),
    )
    return jax.shard_map(
        per_device, mesh=split, in_specs=in_specs, out_specs=P(ROWS, None), check_vma=False
    )
```

time: 473 us -> 172 us (0.36); the launches traced: 468 us -> 172 us
  waiting for transfers between devices: 302 us -> 0 us
  Pallas kernels: 0 us -> 170 us
  matrix products: 94.7 us -> 0 us
  other arithmetic: 33 us -> 0 us
  blocking collectives: 24.2 us -> 0 us
  between operations: 13.5 us -> 0.01 us
    pallas_call x0 -> x1, Pallas kernels: none -> 170 us  [per_device(): pl.pallas_call(whole_kernel, out_shape=jax.ShapeDtypeStruct((32, D), F32)...]
    reduce_scatter x2 -> x0, waiting for transfers between devices: 163 us -> none  [per_device(): mixed = lax.psum_scatter(part, TGT_PLANE, scatter_dimension=0, tiled=True)]
    all_gather x3 -> x0, waiting for transfers between devices: 138 us -> none  [the longest x2 92 us: per_device(): full = lax.all_gather(normed, TGT_PLANE, axis=0, tiled=True)]
    dot_general x8 -> x0, matrix products: 94.7 us -> none  [the longest x2 31.3 us: per_device(): s = jnp.einsum('thd,nd->htn', q, k, preferred_element_type=jnp.float32)]
    reduce_sum x8 -> x0, other arithmetic: 25.4 us -> none  [the longest x2 17.1 us: per_device(): t = jnp.sum(e, axis=-1)]
    all_gather x2 -> x0, blocking collectives: 24.2 us -> none  [per_device(): stats = lax.all_gather(jnp.stack([m, t]), 'z')]
  transfers between devices with their start and end apart: 5 -> 0, of which waited for: 5 -> 0; matrix products, arithmetic and copies ran while one was open for 2% -> 0% of each run, Pallas kernels for 0% -> 0%
where the time goes in v3:
time: 172 us
  Pallas kernels  170 us (99%)
    pallas_call x1, Pallas kernels, per_device(): pl.pallas_call(whole_kernel, out_shape=jax.ShapeDtypeStruct((32, D), F32)...  170 us

profile of v3, /device:TPU:0, one launch (start us, length us, event | category | flops | bytes accessed | tf_op | source)
XLA Modules:
  0.0 171.9 jit_solution(210490034589847516)
XLA Ops:
  0.0 170.2 %whole.1 = f32[32,2048]{1,0:T(8,128)} custom-call(bf16[32,2048]{1,0:T(8,128)(2,1)} %target.1, bf16[64,2048]{1,0:T(8,128)(2,1)} %source.1, bf16[2,2048]{1,0:T(2,128)(2,1)} %target_gain.1, bf16[2,2048]{1,0:T(2,128)(2,1)} %source_gain.1, f32[2,2]{1,0:T(2,128)} %head_temp.1, bf16[2048]{0:T(1024)(128)(2,1)} %final_gain.1, bf16[2,2048,1024]{2,1,0:T(8,128)(2,1)} %query_w.1, ...), custom_call_target="tpu_custom_call" | custom-call | tf_op jit(solution)/shard_map/whole/pallas_call | solution.py:597
  170.2 1.7 copy.12

commit v4 on v2

--- a/solution.py
+++ b/solution.py
@@ -69,6 +69,18 @@
     return (1, 0) if o == 1 else (-1, 0)
 
 
+def below(h, i, j):
+    labels = [(i, o) for way, o in line_sends(h, j)]
+    if j == 0:
+        labels += [(o, 0) for way, o in line_sends(h, i)]
+    return labels
+
+
+JOINS = [
+    (h, i, j) for h in range(GROUPS) for i in range(RING) for j in range(RING) if below(h, i, j)
+]
+
+
 class Here:
     def __init__(self):
         self.at = {a: lax.axis_index(a) for a in ROWS}
@@ -100,22 +112,27 @@
 
 
 class Gather:
-    def __init__(self, here, ref, order, sems):
-        self.here, self.ref, self.order = here, ref, order
-        self.ring_send, self.ring_recv, self.sib_send, self.sib_recv = sems
-        self.sent = []
+    def __init__(self, here, ref, bulk, order, sems):
+        self.here, self.ref, self.bulk, self.order = here, ref, bulk, order
+        self.send, self.ring_recv, self.sib_recv = sems
+        self.sent = 0
 
     def ring(self, h, src, dst, axis, way):
-        n = piece_no(h, *dst)
-        return pltpu.make_async_remote_copy(
-            self.ref(0, h, *src), self.ref(0, h, *dst), self.ring_send.at[n], self.ring_recv.at[n],
+        r = AWAY[dst[0]] + AWAY[dst[1]]
+        return pltpu.make_async_remote_copy(
+            self.ref(0, h, *src), self.ref(0, h, *dst), self.send.at[0], self.ring_recv.at[(r - 1) * GROUPS + h],
             device_id=self.here.next(axis, way), device_id_type=MESH,
         )
 
     def sib(self, h, i, j):
-        n = piece_no(h, i, j)
-        return pltpu.make_async_remote_copy(
-            self.ref(0, h, i, j), self.ref(1, h, i, j), self.sib_send.at[n], self.sib_recv.at[n],
+        return pltpu.make_async_remote_copy(
+            self.ref(0, h, i, j), self.ref(1, h, i, j), self.send.at[0], self.sib_recv.at[AWAY[i] + AWAY[j]],
+            device_id=self.here.sibling(), device_id_type=MESH,
+        )
+
+    def whole(self, n, recv):
+        return pltpu.make_async_remote_copy(
+            self.bulk(n), self.bulk(n), self.send.at[0], recv,
             device_id=self.here.sibling(), device_id_type=MESH,
         )
 
@@ -126,26 +143,23 @@
             copies += [self.ring(h, (i, 0), (o, 0), first, way) for way, o in line_sends(h, i)]
         copies += [self.ring(h, (i, j), (i, o), second, way) for way, o in line_sends(h, j)]
         copies.append(self.sib(h, i, j))
-        self.sent += start_all(copies)
+        self.sent += len(start_all(copies))
 
     def spread_own(self):
         for h in range(GROUPS):
             self.spread(h, 0, 0)
 
     def relay(self, r, h):
+        self.whole(len(ROUNDS[r]), self.ring_recv.at[(r - 1) * GROUPS + h]).wait_recv()
         for i, j in ROUNDS[r]:
-            self.ring(h, (0, 0), (i, j), "x", 1).wait_recv()
             self.spread(h, i, j)
 
     def arrive_sib(self, r):
-        for h in range(GROUPS):
-            for i, j in ROUNDS[r]:
-                self.sib(h, i, j).wait_recv()
+        self.whole(len(ROUNDS[r]) * GROUPS, self.sib_recv.at[r]).wait_recv()
 
     def finish(self):
-        for copy in self.sent:
-            copy.wait_send()
-        self.sent = []
+        self.whole(self.sent, self.sib_recv.at[0]).wait_send()
+        self.sent = 0
 
 
 def source_ref(src):
@@ -153,6 +167,10 @@
         return src.at[pl.ds(SRC_SLOT[piece] * SRC_PIECE, SRC_PIECE), :]
 
     return ref
+
+
+def source_bulk(src):
+    return lambda n: src.at[pl.ds(0, n * SRC_PIECE), :]
 
 
 def place_of(order, h, i, j):
@@ -168,6 +186,15 @@
     return ref
 
 
+def target_bulk(tgt):
+    def bulk(n):
+        if n <= 64:
+            return tgt.at[pl.ds(0, n * TGT_PIECE), pl.ds(0, 1024)]
+        return tgt.at[pl.ds(0, n * TGT_PIECE // 2), :]
+
+    return bulk
+
+
 def unit_times(values, gain):
     scale = lax.rsqrt(jnp.mean(values * values, axis=-1, keepdims=True) + EPS)
     return values * scale * gain.astype(F32)
@@ -178,8 +205,7 @@
     result,
     src, tgt, kv_w, q_w, kv_buf, q_buf, g_buf,
     w_buf, e_buf, o_buf, p_buf, att, att_out, ring_out, ring_in, st_own, st_in, hidden,
-    s_ring_send, s_ring_recv, s_sib_send, s_sib_recv,
-    t_ring_send, t_ring_recv, t_sib_send, t_sib_recv,
+    s_send, s_ring_recv, s_sib_recv, t_send, t_ring_recv, t_sib_recv,
     load_sem, st_send, st_recv, sib_send, sib_recv, ring_send, ring_recv,
 ):
     here = Here()
@@ -252,37 +278,37 @@
     greet(
         [here.next(a, k) for a in "xyz" for k in (1, -1)] + [here.next("z", 2), here.sibling()]
     )
-    sg = Gather(here, source_ref(src), XY, (s_ring_send, s_ring_recv, s_sib_send, s_sib_recv))
-    tg = Gather(here, target_ref(tgt, XX), XX, (t_ring_send, t_ring_recv, t_sib_send, t_sib_recv))
+    sg = Gather(here, source_ref(src), source_bulk(src), XY, (s_send, s_ring_recv, s_sib_recv))
+    tg = Gather(here, target_ref(tgt, XX), target_bulk(tgt), XX, (t_send, t_ring_recv, t_sib_recv))
     sg.spread_own()
     tg.spread_own()
     out_sib = out_share(0)
     out_sib.start()
     spread_ratio()
     wait_all(weights)
+    for h in range(GROUPS):
+        tg.relay(1, h)
     for r in range(1, 5):
         for h in range(GROUPS):
-            tg.relay(r, h)
-            sg.relay(r, h)
+            if r < 4:
+                tg.relay(r + 1, h)
+            if r < 4 or h == 0:
+                sg.relay(r, h)
             if h == 0:
                 sg.arrive_sib(r - 1)
                 tg.arrive_sib(r - 1)
             if r == 2 and h % 2 == 1:
                 project_kv(0, 640, h // 2)
-            if r == 3 and h == 0:
-                project_kv(640, 384, 0)
-            if r == 3 and h == 1:
-                project_kv(640, 384, 1)
-            if r == 3 and h == 2:
-                project_kv(1024, 384, 0)
-            if r == 3 and h == 3:
-                project_kv(1024, 384, 1)
+            if r == 3:
+                project_kv(640 + 384 * (h // 2), 384, h % 2)
             if r == 4 and h == 0:
                 project_q(0)
     project_q(1)
     project_q(3)
     tg.arrive_sib(4)
     project_q(2)
+    for h in range(1, GROUPS):
+        sg.relay(4, h)
     sg.arrive_sib(4)
     project_kv(1408, 640, 0)
     project_kv(1408, 640, 1)
@@ -306,7 +332,7 @@
         place_target(hidden[...], 1)
         out_own = out_load(1)
         out_own.start()
-        tg = Gather(here, target_ref(tgt, XZ), XZ, (t_ring_send, t_ring_recv, t_sib_send, t_sib_recv))
+        tg = Gather(here, target_ref(tgt, XZ), target_bulk(tgt), XZ, (t_send, t_ring_recv, t_sib_recv))
         tg.spread_own()
         for r in range(1, 5):
             for h in range(GROUPS):
@@ -404,32 +430,39 @@
         lax.fori_loop(0, 4, body, 0)
 
     def ring_copy(h, i, j):
-        axis, way = (XZ[h][1], line_up(h, j)[0]) if j else (XZ[h][0], line_up(h, i)[0])
+        if j:
+            way, up = line_up(h, j)
+            axis, parent = XZ[h][1], (i, up)
+        else:
+            way, up = line_up(h, i)
+            axis, parent = XZ[h][0], (up, 0)
         n = piece_no(h, i, j)
         return pltpu.make_async_remote_copy(
-            ring_out.at[n], ring_in.at[n], ring_send.at[n], ring_recv.at[n],
+            ring_out.at[n], ring_in.at[n], ring_send.at[0], ring_recv.at[JOINS.index((h, *parent))],
             device_id=here.next(axis, way), device_id_type=MESH,
         )
 
-    def below(h, i, j):
-        labels = [(i, o) for way, o in line_sends(h, j)]
-        if j == 0:
-            labels += [(o, 0) for way, o in line_sends(h, i)]
-        return labels
+    def ring_bulk(n, recv):
+        return pltpu.make_async_remote_copy(
+            ring_out.at[0:n], ring_in.at[0:n], ring_send.at[0], recv,
+            device_id=here.sibling(), device_id_type=MESH,
+        )
 
     def collect(h, i, j):
         zd, xd = place_of(XZ, h, i, j)
         pair, at = PAIR[zd]
         rows = pl.ds(at * 128 + ((h % 2) * 4 + xd) * 16, 16)
         value = p_buf[pair, rows, pl.ds((h // 2) * 1024, 1024)]
-        for label in below(h, i, j):
-            ring_copy(h, *label).wait_recv()
+        labels = below(h, i, j)
+        if labels:
+            ring_bulk(len(labels), ring_recv.at[JOINS.index((h, i, j))]).wait_recv()
+        for label in labels:
             value += ring_in[piece_no(h, *label)].astype(F32)
         return value
 
     def pass_on(h, i, j):
         ring_out[piece_no(h, i, j)] = collect(h, i, j).astype(BF16)
-        pending.extend(start_all([ring_copy(h, i, j)]))
+        ring_copy(h, i, j).start()
 
     passed = set()
 
@@ -479,10 +512,11 @@
         value = jnp.concatenate([collect(half, 0, 0), collect(half + 2, 0, 0)], axis=1)
         value += before[at, :].astype(F32)
         if final_gain is not None:
-            value = unit_times(value, final_gain[...])
+            value = unit_times(value, final_gain[...][None, :])
         after[at, :] = value
     for copy in pending:
         copy.wait_send()
+    ring_bulk(15 * GROUPS, ring_recv.at[0]).wait_send()
 
 
 def vmem(*shape, dtype=BF16):
@@ -508,12 +542,14 @@
             vmem(2048, D), vmem(4, 512, 2048), vmem(2, 512, HEAD_DIM, dtype=F32), vmem(2, 256, D, dtype=F32),
             vmem(2, 256, D), vmem(4, 128, 1024), vmem(64, 16, 1024), vmem(64, 16, 1024),
             vmem(4, 8, 512, dtype=F32), vmem(3, 4, 8, 512, dtype=F32), vmem(32, D, dtype=F32),
-        ] + [DMA((64,))] * 8 + [DMA((4,)), DMA((3,)), DMA((3,)), DMA((5,)), DMA((5,)), DMA((64,)), DMA((64,))],
+        ] + [DMA((1,)), DMA((16,)), DMA((5,))] * 2 + [
+            DMA((4,)), DMA((3,)), DMA((3,)), DMA((5,)), DMA((5,)), DMA((1,)), DMA((len(JOINS),)),
+        ],
         compiler_params=pltpu.CompilerParams(
             collective_id=0, has_side_effects=True, vmem_limit_bytes=VMEM_LIMIT
         ),
         name="whole",
-    )(target, source, target_gain, source_gain, head_temp, final_gain.reshape(1, D), query_w, key_w, value_w, out_w)
+    )(target, source, target_gain, source_gain, head_temp, final_gain, query_w, key_w, value_w, out_w)
 
 
 def solution(mesh):

time: 152 us -> 149 us (0.980)
  no operation moved by 1% of the time
where the time goes in v4:
time: 149 us
  Pallas kernels  147 us (99%)
  local copies, waits for them, and re-layouts  1.67 us (1%)
    pallas_call x1, Pallas kernels, per_device(): pl.pallas_call(whole_kernel, out_shape=jax.ShapeDtypeStruct((32, D), F32)...  147 us

profile of v4, /device:TPU:0, one launch (start us, length us, event | category | flops | bytes accessed | tf_op | source)
XLA Modules:
  0.0 148.8 jit_solution(11231244941239195783)
XLA Ops:
  0.0 147.1 %whole.1 = f32[32,2048]{1,0:T(8,128)} custom-call(bf16[32,2048]{1,0:T(8,128)(2,1)} %target.1, bf16[64,2048]{1,0:T(8,128)(2,1)} %source.1, bf16[2,2048]{1,0:T(2,128)(2,1)} %target_gain.1, bf16[2,2048]{1,0:T(2,128)(2,1)} %source_gain.1, f32[2,2]{1,0:T(2,128)} %head_temp.1, bf16[2048]{0:T(1024)(128)(2,1)} %final_gain.1, bf16[2,2048,1024]{2,1,0:T(8,128)(2,1)} %query_w.1, ...), custom_call_target="tpu_custom_call" | custom-call | tf_op jit(solution)/shard_map/whole/pallas_call | solution.py:534
  147.1 1.7 %copy.12 = f32[32,2048]{1,0:T(8,128)} copy(f32[32,2048]{1,0:T(8,128)} %whole.1) | data formatting | bytes 524288
